TPU v7x, 32 devices: a whole 2x2x4 slice. The times are simulated.
32 devices in a mesh: ep: 8 (over z, x), tp: 4 (over y, core).
Axes of the slice: x: 2, y: 2, z: 4, core: 2. Of those that a mesh axis runs over, the one named last changes fastest.
Arguments:
- tokens: bfloat16 [1024, 4096], P('ep', 'tp'), may hold values from -6 to 6
- cotangent: bfloat16 [1024, 4096], P('ep', 'tp'), may hold values from -6 to 6
- routes: int32 [1024, 2], P('ep'), may hold values from 0 to 7, all different within a row; in each aligned block of 128 rows (0 to 127, 128 to 255, ...) at most 48 rows name the same one
- gate_weight: float32 [1024, 2], P('ep'), may hold values from 0.1 to 2.5
- w_gate: bfloat16 [8, 1024, 4096], P('ep', 'tp'), may hold values from -0.09375 to 0.09375
- w_up: bfloat16 [8, 1024, 4096], P('ep', 'tp'), may hold values from -0.09375 to 0.09375
- w_down: bfloat16 [8, 1024, 4096], P('ep', 'tp'), may hold values from -0.1875 to 0.1875
- shared_hidden: bfloat16 [1024, 1024], P('ep'), may hold values from -4 to 4
Outputs:
- tokens_grad: bfloat16 [1024, 4096], P('ep', 'tp')
- gate_grad: float32 [1024, 2], P('ep')
- w_gate_grad: float32 [8, 1024, 4096], P('ep', 'tp')
- w_up_grad: float32 [8, 1024, 4096], P('ep', 'tp')
- w_down_grad: float32 [8, 1024, 4096], P('ep', 'tp')
- shared_grad: float32 [1024, 4096], P('ep', 'tp')
Inputs may be any that keep to these rules, and one draw needn't show every extreme that they name: `routes`: each row names 2 different experts. Among the rows of one index of ep (aligned blocks of 128 rows) no expert is named more than 48 times, and in every draw some expert is named exactly 48 times in some block.
All inputs are finite; a program needn't handle non-finite values.
Results may differ from a plain program's by a relative error of at most 0.022.
Values may be sent and summed in bfloat16 or wider, within the bound.
A program may use at most 64 MiB of HBM per device.

v0:
```python
import jax
import jax.numpy as jnp
from jax import lax
from jax.sharding import PartitionSpec as P


def slot_positions(flat_routes, experts):
    onehot = (flat_routes[:, None] == jnp.arange(experts, dtype=jnp.int32)[None, :]).astype(
        jnp.int32
    )
    earlier = jnp.cumsum(onehot, axis=0) - onehot
    return jnp.sum(earlier * onehot, axis=1)


def shards(tokens, cotangent, routes, gate_weight, w_gate, w_up, w_down, shared_hidden):
    tok_count, top_count = routes.shape
    experts = lax.axis_size("ep")
    capacity = 3 * tok_count * top_count // (2 * experts)
    flat_routes = routes.reshape(-1)
    positions = slot_positions(flat_routes, experts)
    token_ids = jnp.arange(tok_count * top_count, dtype=jnp.int32) // top_count
    slot_table = (
        jnp.full((experts, capacity), tok_count, jnp.int32)
        .at[flat_routes, positions]
        .set(token_ids)
    )
    weight_table = (
        jnp.zeros((experts, capacity), jnp.float32)
        .at[flat_routes, positions]
        .set(gate_weight.reshape(-1))
    )

    def place_rows(source_rows):
        padded = jnp.concatenate(
            [source_rows, jnp.zeros((1, source_rows.shape[1]), source_rows.dtype)], 0
        )
        return padded[slot_table]

    part_tokens, part_cotan, recv_weight = (
        lax.all_to_all(place_rows(tokens), "ep", split_axis=0, concat_axis=0, tiled=True),
        lax.all_to_all(place_rows(cotangent), "ep", split_axis=0, concat_axis=0, tiled=True),
        lax.all_to_all(
            weight_table.astype(jnp.bfloat16), "ep", split_axis=0, concat_axis=0, tiled=True
        ).astype(weight_table.dtype),
    )
    recv_tokens, recv_cotan = (
        lax.all_gather(part_tokens, "tp", axis=2, tiled=True),
        lax.all_gather(part_cotan, "tp", axis=2, tiled=True),
    )
    row_total = experts * capacity
    width = recv_tokens.shape[2]
    contract_last = (((1,), (1,)), ((), ()))
    rows_x = recv_tokens.reshape(row_total, width)
    rows_g = recv_cotan.reshape(row_total, width)
    weight_col = recv_weight.reshape(row_total, 1)
    gate_mat = w_gate[0]
    up_mat = w_up[0]
    down_mat = w_down[0]
    pre_gate = lax.dot_general(rows_x, gate_mat, contract_last, preferred_element_type=jnp.float32)
    pre_up = lax.dot_general(rows_x, up_mat, contract_last, preferred_element_type=jnp.float32)
    sigmoid_gate = jax.nn.sigmoid(pre_gate)
    silu_gate = pre_gate * sigmoid_gate
    hidden = (silu_gate * pre_up).astype(jnp.bfloat16)
    back_hidden = lax.dot_general(
        rows_g, down_mat, contract_last, preferred_element_type=jnp.float32
    )
    gate_part = jnp.sum(hidden.astype(jnp.float32) * back_hidden, axis=1)
    scaled = weight_col * back_hidden
    grad_pre_gate = (
        scaled * pre_up * sigmoid_gate * (1.0 + pre_gate * (1.0 - sigmoid_gate))
    ).astype(jnp.bfloat16)
    grad_pre_up = (scaled * silu_gate).astype(jnp.bfloat16)
    weighted_cotan = (weight_col * rows_g.astype(jnp.float32)).astype(jnp.bfloat16)
    grad_down = jnp.dot(hidden.T, weighted_cotan, preferred_element_type=jnp.float32)
    grad_gate = jnp.dot(grad_pre_gate.T, rows_x, preferred_element_type=jnp.float32)
    grad_up = jnp.dot(grad_pre_up.T, rows_x, preferred_element_type=jnp.float32)
    partial_value = jnp.dot(grad_pre_gate, gate_mat, preferred_element_type=jnp.float32)
    partial_value = partial_value + jnp.dot(grad_pre_up, up_mat, preferred_element_type=jnp.float32)
    rounded = lax.optimization_barrier(partial_value.astype(jnp.bfloat16)).astype(jnp.float32)
    row_share = lax.psum_scatter(
        rounded.reshape(experts, capacity, width).astype(jnp.bfloat16),
        "tp",
        scatter_dimension=2,
        tiled=True,
    )
    gate_total = lax.psum(gate_part.reshape(experts, capacity), "tp")
    back_rows, back_gate = (
        lax.all_to_all(row_share, "ep", split_axis=0, concat_axis=0, tiled=True),
        lax.all_to_all(
            gate_total.astype(jnp.bfloat16), "ep", split_axis=0, concat_axis=0, tiled=True
        ).astype(gate_total.dtype),
    )
    picked = back_rows[flat_routes, positions].astype(jnp.float32)
    tokens_grad = jnp.sum(picked.reshape(tok_count, top_count, -1), axis=1).astype(jnp.bfloat16)
    gate_grad = back_gate[flat_routes, positions].reshape(tok_count, top_count)
    shared_grad = lax.psum_scatter(
        jnp.dot(shared_hidden.T, cotangent, preferred_element_type=jnp.float32).astype(
            jnp.bfloat16
        ),
        "ep",
        scatter_dimension=0,
        tiled=True,
    ).astype(jnp.float32)
    return (tokens_grad, gate_grad, grad_gate[None], grad_up[None], grad_down[None], shared_grad)


def solution(mesh):
    placed = (
        P("ep", "tp"),
        P("ep", "tp"),
        P("ep", None),
        P("ep", None),
        P("ep", "tp", None),
        P("ep", "tp", None),
        P("ep", "tp", None),
        P("ep", None),
    )
    return jax.shard_map(
        shards,
        mesh=mesh,
        in_specs=placed,
        out_specs=(
            P("ep", "tp"),
            P("ep", None),
            P("ep", "tp", None),
            P("ep", "tp", None),
            P("ep", "tp", None),
            P("ep", "tp"),
        ),
        check_vma=False,
    )
```

profile of v0, /device:TPU:0, one launch (start us, length us, event | category | flops | bytes accessed | tf_op | source)
XLA Modules:
  0.0 263.4 jit_solution(10906129035726146199)
XLA Ops:
  7.2 0.0 copy-start
  7.2 0.0 all-gather.5.cloned.1.call-start
  7.2 0.9 copy.26
  8.2 0.1 eq.29
  8.3 0.1 eq.25
  8.4 0.1 reshape.106
  8.6 0.6 reduce-window.6
  9.2 0.2 slice_reduce_fusion
  9.4 0.1 fusion.12
  9.6 11.2 %scatter_fusion.1 = s32[8,48]{1,0:T(8,128)S(1)} fusion(s32[8,48]{1,0:T(8,128)S(1)} %broadcast_in_dim.13, s32[256]{0:T(256)S(1)} %bitcast.57, s32[256]{0:T(256)S(1)} %and_select_fusion), kind=kCustom, calls=%fused_computation.5 | custom fusion | bytes 5120 | tf_op jit(solution)/shard_map/scatter | solution.py:25
  20.8 0.1 reshape.117
  20.9 1.0 concatenate.14
  21.8 0.0 copy-start.6
  21.9 2.1 gather_fusion.1
  23.9 27.3 %all_to_all.33 = bf16[8,48,1024]{2,1,0:T(8,128)(2,1)} all-to-all(bf16[8,48,1024]{2,1,0:T(8,128)(2,1)S(1)} %bitcast.67), channel_id=1, replica_groups=mesh['ep'=8,'tp'=4] {'ep'}, dimensions={0} | all-to-all | bytes 1572864 | tf_op jit(solution)/shard_map/all_to_all | solution.py:40
  51.3 0.0 all-gather.5.cloned.1.call-update
  51.3 0.0 all-gather.3.cloned.1.call-start
  51.3 0.0 copy-done.6
  51.4 0.0 copy-start.9
  51.4 2.1 gather_fusion
  53.5 23.3 %all_to_all.34 = bf16[8,48,1024]{2,1,0:T(8,128)(2,1)} all-to-all(bf16[8,48,1024]{2,1,0:T(8,128)(2,1)S(1)} %bitcast.66), channel_id=1, replica_groups=mesh['ep'=8,'tp'=4] {'ep'}, dimensions={0} | all-to-all | bytes 1572864 | tf_op jit(solution)/shard_map/all_to_all | solution.py:41
  76.8 0.0 all-gather.3.cloned.1.call-update
  76.8 0.0 reduce-scatter.3.cloned.1.call-start
  76.8 0.0 copy-done.9
  76.9 0.1 copy.29
  77.0 0.1 reshape.145
  77.1 11.2 %scatter_fusion = f32[8,48]{1,0:T(8,128)S(1)} fusion(f32[8,48]{1,0:T(8,128)S(1)} %broadcast_in_dim.12, s32[256]{0:T(256)S(1)} %bitcast.58, f32[256]{0:T(256)S(1)} %reshape.145), kind=kCustom, calls=%fused_computation.4 | custom fusion | bytes 5120 | tf_op jit(solution)/shard_map/scatter | solution.py:30
  88.3 9.9 %all_to_all.35 = bf16[8,1,48]{2,1,0:T(2,128)(2,1)S(1)} all-to-all(bf16[8,1,48]{2,1,0:T(2,128)(2,1)S(1)} %copy.30), channel_id=1, replica_groups=mesh['ep'=8,'tp'=4] {'ep'}, dimensions={0} | all-to-all | bytes 1536 | tf_op jit(solution)/shard_map/all_to_all | solution.py:42
  98.2 0.1 reshape.113
  98.3 0.0 copy-start.1
  98.3 0.0 copy-start.4
  98.4 0.0 copy-done
  98.4 3.3 %fusion.3 = f32[384,256]{0,1:T(8,128)S(1)} fusion(bf16[384,4096]{1,0:T(8,128)(2,1)} %bitcast.61, bf16[1,256,4096]{2,1,0:T(8,128)(2,1)S(1)} %copy-done), kind=kOutput, calls=%fused_computation.14 | convolution fusion | flops 805306368 | bytes 5636096 | tf_op jit(solution)/shard_map/dot_general | solution.py:59
  101.7 0.0 copy-done.1
  101.7 0.2 copy-done.4
  101.9 2.0 fusion.6
  103.9 5.2 %all-gather.3.cloned.1.call-done = bf16[8,48,4096]{2,1,0:T(8,128)(2,1)} async-done(((bf16[8,48,1024]{2,1,0:T(8,128)(2,1)}), bf16[8,48,4096]{2,1,0:T(8,128)(2,1)}) %all-gather.3.cloned.1.call-update) | async-done | bytes 3145744 | tf_op jit(solution)/shard_map/all_gather | solution.py:48
  109.1 4.6 %multiply_reduce_fusion = (f32[384]{0:T(512)S(1)}, bf16[384,256]{0,1:T(8,128)(2,1)}, bf16[384,256]{0,1:T(8,128)(2,1)S(1)}, bf16[384,256]{0,1:T(8,128)(2,1)S(1)}) fusion(f32[384,256]{0,1:T(8,128)} %fusion.6, f32[384,256]{0,1:T(8,128)S(1)} %fusion.3, f32[384]{0:T(512)S(1)} %reshape.113, bf16[384,4096]{1,0:T(8,128)(2,1)} %bitcast.68, ...), kind=kOutput, calls=%fused_computation.22 | convolution fusion | flops 807173760 | bytes 6622208 | tf_op jit(solution)/shard_map/dot_general | solution.py:64
  113.7 1.0 fusion.1
  114.7 0.6 copy-done.5
  115.3 2.7 %add_convert_fusion = bf16[384,4096]{1,0:T(8,128)(2,1)} fusion(f32[384,4096]{1,0:T(8,128)S(1)} %fusion.1, bf16[384,256]{0,1:T(8,128)(2,1)S(1)} %get-tuple-element.29, bf16[1,256,4096]{2,1,0:T(8,128)(2,1)S(1)} %copy-done.5), kind=kOutput, calls=%fused_computation.7 | convolution fusion | flops 808452096 | bytes 11730944 | tf_op jit(solution)/shard_map/dot_general | solution.py:78
  118.0 0.0 reduce-scatter.3.cloned.1.call-update
  118.0 0.0 reduce-scatter.5.cloned.1.call-start
  118.1 0.9 copy-done.7
  119.0 2.1 convolution_convert_fusion
  121.0 0.0 reduce-scatter.5.cloned.1.call-update
  121.0 0.1 reshape.111
  121.1 5.9 %psum.7 = bf16[8,48]{1,0:T(8,128)(2,1)S(1)} all-reduce(f32[8,48]{1,0:T(8,128)S(1)} %reshape.111), channel_id=1, replica_groups=mesh['ep'=8,'tp'=4] {'tp'}, use_global_device_ids=true, to_apply=%region_8.9 | all-reduce | flops 384 | bytes 2304 | tf_op jit(solution)/shard_map/psum | solution.py:86
  127.0 11.9 %all_to_all.36 = bf16[8,1,48]{2,1,0:T(2,128)(2,1)S(1)} all-to-all(bf16[8,1,48]{2,1,0:T(2,128)(2,1)S(1)} %copy.31), channel_id=1, replica_groups=mesh['ep'=8,'tp'=4] {'ep'}, dimensions={0} | all-to-all | bytes 1536 | tf_op jit(solution)/shard_map/all_to_all | solution.py:89
  138.9 17.0 %reduce-scatter.3.cloned.1.call-done = bf16[8,48,1024]{2,1,0:T(8,128)(2,1)} async-done(((bf16[8,48,4096]{2,1,0:T(8,128)(2,1)}), bf16[8,48,1024]{2,1,0:T(8,128)(2,1)}) %reduce-scatter.3.cloned.1.call-update) | async-done | bytes 786448 | tf_op jit(solution)/shard_map/reduce_scatter | solution.py:80
  155.9 5.5 %all-to-all-start.3 = ((bf16[8,48,1024]{2,1,0:T(8,128)(2,1)}), bf16[8,48,1024]{2,1,0:T(8,128)(2,1)S(1)}, u32[]{:S(2)}, u32[]{:S(2)}) async-start(bf16[8,48,1024]{2,1,0:T(8,128)(2,1)} %reduce-scatter.3.cloned.1.call-done), calls=%async_computation.4 | async-start | bytes 1572864 | tf_op jit(solution)/shard_map/all_to_all | solution.py:88
  161.4 74.3 %reduce-scatter.5.cloned.1.call-done = bf16[128,1024]{1,0:T(8,128)(2,1)} async-done(((bf16[1024,1024]{1,0:T(8,128)(2,1)}), bf16[128,1024]{1,0:T(8,128)(2,1)}) %reduce-scatter.5.cloned.1.call-update) | async-done | bytes 262160 | tf_op jit(solution)/shard_map/reduce_scatter | solution.py:96
  235.7 1.8 convert_element_type.81
  237.5 5.3 %convolution_bitcast_fusion.1 = f32[1,256,4096]{2,1,0:T(8,128)} fusion(bf16[384,256]{0,1:T(8,128)(2,1)S(1)} %get-tuple-element.29, bf16[384,4096]{1,0:T(8,128)(2,1)} %bitcast.62), kind=kOutput, calls=%fused_computation.9 | convolution fusion | flops 805306368 | bytes 7536640 | tf_op jit(solution)/shard_map/dot_general | solution.py:76
  242.9 0.0 copy-done.2
  242.9 3.3 %convolution_bitcast_fusion.2 = f32[1,256,4096]{2,1,0:T(8,128)} fusion(bf16[384,256]{0,1:T(8,128)(2,1)S(1)} %get-tuple-element.28, bf16[384,4096]{1,0:T(8,128)(2,1)S(1)} %bitcast.64), kind=kOutput, calls=%fused_computation.10 | convolution fusion | flops 805306368 | bytes 7536640 | tf_op jit(solution)/shard_map/dot_general | solution.py:75
  246.2 3.4 %convolution_bitcast_fusion = f32[1,256,4096]{2,1,0:T(8,128)} fusion(bf16[384,256]{0,1:T(8,128)(2,1)S(1)} %copy-done.8, bf16[384,4096]{1,0:T(8,128)(2,1)S(1)} %bitcast.69, f32[384]{0:T(512)S(1)} %reshape.113), kind=kOutput, calls=%fused_computation.8 | convolution fusion | flops 810024960 | bytes 7538176 | tf_op jit(solution)/shard_map/dot_general | solution.py:74
  249.6 1.4 gather_fusion.3
  251.0 0.1 reshape.112
  251.1 0.6 copy.33
  251.8 0.0 all-to-all-done.3
  251.8 2.8 %gather_fusion.2 = bf16[256,1024]{1,0:T(8,128)(2,1)S(1)} fusion(bf16[8,48,1024]{2,1,0:T(8,128)(2,1)S(1)} %all-to-all-done.3, s32[256]{0:T(256)S(1)} %bitcast.60), kind=kCustom, calls=%fused_computation.2 | custom fusion | bytes 1050624 | tf_op jit(solution)/shard_map/gather | solution.py:93
  254.5 0.2 gather.17
  254.7 2.1 reduce_sum.34
  (23 shorter events, 0.1 us)
Async XLA Ops:
  7.2 91.2 %copy-start = (bf16[1,256,4096]{2,1,0:T(8,128)(2,1)S(1)}, bf16[1,256,4096]{2,1,0:T(8,128)(2,1)}, u32[]{:S(2)}) copy-start(bf16[1,256,4096]{2,1,0:T(8,128)(2,1)} %param.12) | copy-start | bytes 6291460
  7.2 91.1 %all-gather.5.cloned.1.call-start = ((), (), s32[]{:S(2)}) async-start(), calls=%async_computation.8 | async-start | bytes 3932160 | tf_op jit(solution)/shard_map/all_gather | solution.py:47
  21.8 29.5 %copy-start.6 = (bf16[128,1024]{1,0:T(8,128)(2,1)S(1)}, bf16[128,1024]{1,0:T(8,128)(2,1)}, u32[]{:S(2)}) copy-start(bf16[128,1024]{1,0:T(8,128)(2,1)} %param.9) | copy-start | bytes 786436
  51.3 57.8 %all-gather.3.cloned.1.call-start = ((), (), s32[]{:S(2)}) async-start(), calls=%async_computation.7 | async-start | bytes 3932160 | tf_op jit(solution)/shard_map/all_gather | solution.py:48
  51.4 25.5 %copy-start.9 = (f32[128,2]{0,1:T(2,128)S(1)}, f32[128,2]{0,1:T(2,128)}, u32[]{:S(2)}) copy-start(f32[128,2]{0,1:T(2,128)} %param.11) | copy-start | bytes 3076
  76.8 79.1 %reduce-scatter.3.cloned.1.call-start = ((), (), s32[]{:S(2)}) async-start(), calls=%async_computation.9 | async-start | bytes 3932160 | tf_op jit(solution)/shard_map/reduce_scatter | solution.py:80
  98.3 3.3 %copy-start.1 = (bf16[8,48,4096]{2,1,0:T(8,128)(2,1)S(1)}, bf16[8,48,4096]{2,1,0:T(8,128)(2,1)}, u32[]{:S(2)}) copy-start(bf16[8,48,4096]{2,1,0:T(8,128)(2,1)} %all-gather.5.cloned.1.call-done) | copy-start | bytes 9437188
  98.3 3.5 %copy-start.4 = (bf16[1,256,4096]{2,1,0:T(8,128)(2,1)S(1)}, bf16[1,256,4096]{2,1,0:T(8,128)(2,1)}, u32[]{:S(2)}) copy-start(bf16[1,256,4096]{2,1,0:T(8,128)(2,1)} %param.13) | copy-start | bytes 6291460
  113.7 1.6 copy-start.5
  118.0 0.9 copy-start.7
  118.0 117.7 %reduce-scatter.5.cloned.1.call-start = ((), (), s32[]{:S(2)}) async-start(), calls=%async_computation.10 | async-start | bytes 2359296 | tf_op jit(solution)/shard_map/reduce_scatter | solution.py:96
  155.9 95.8 %all-to-all-start.3 = ((bf16[8,48,1024]{2,1,0:T(8,128)(2,1)}), bf16[8,48,1024]{2,1,0:T(8,128)(2,1)S(1)}, u32[]{:S(2)}, u32[]{:S(2)}) async-start(bf16[8,48,1024]{2,1,0:T(8,128)(2,1)} %reduce-scatter.3.cloned.1.call-done), calls=%async_computation.4 | async-start | bytes 1572864 | tf_op jit(solution)/shard_map/all_to_all | solution.py:88
  237.5 5.3 %copy-start.2 = (bf16[8,48,4096]{2,1,0:T(8,128)(2,1)S(1)}, bf16[8,48,4096]{2,1,0:T(8,128)(2,1)}, u32[]{:S(2)}) copy-start(bf16[8,48,4096]{2,1,0:T(8,128)(2,1)} %all-gather.5.cloned.1.call-done) | copy-start | bytes 9437188
  242.9 3.3 %copy-start.3 = (bf16[8,48,4096]{2,1,0:T(8,128)(2,1)S(1)}, bf16[8,48,4096]{2,1,0:T(8,128)(2,1)}, u32[]{:S(2)}) copy-start(bf16[8,48,4096]{2,1,0:T(8,128)(2,1)} %all-gather.3.cloned.1.call-done) | copy-start | bytes 9437188
  242.9 3.3 %copy-start.8 = (bf16[384,256]{0,1:T(8,128)(2,1)S(1)}, bf16[384,256]{0,1:T(8,128)(2,1)}, u32[]{:S(2)}) copy-start(bf16[384,256]{0,1:T(8,128)(2,1)} %get-tuple-element.25) | copy-start | bytes 589828
Sparse Core Ops, SparseCore 0:
  51.4 27.5 all-gather.4
  80.6 28.5 all-gather.2
  118.1 37.7 reduce-scatter.2
  159.9 75.7 reduce-scatter.4
where the time goes:
time: 264 us; the launch traced here: 263 us
  waiting for transfers between devices  96.6 us (37%)
  blocking collectives  78.3 us (30%)
  local copies, waits for them, and re-layouts  36.4 us (14%)
  matrix products  27.7 us (10%)
  between operations  14 us (5%)
  starting transfers between devices  5.68 us (2%)
  other arithmetic  4.71 us (2%)
    reduce_scatter x1, waiting for transfers between devices, shards(): lax.psum_scatter(jnp.dot(shared_hidden.T, cotangent, preferred_element_ty...  74.3 us
    all_to_all x1, blocking collectives, shards(): lax.all_to_all(place_rows(tokens), 'ep', split_axis=0, concat_axis=0, til...  27.3 us
    all_to_all x1, blocking collectives, shards(): lax.all_to_all(place_rows(cotangent), 'ep', split_axis=0, concat_axis=0,...  23.3 us
    reduce_scatter x1, waiting for transfers between devices, shards(): lax.psum_scatter(rounded.reshape(experts, capacity, width).astype(jnp.bfl...  17 us
    all_to_all x1, blocking collectives, shards(): lax.all_to_all(gate_total.astype(jnp.bfloat16), 'ep', split_axis=0, conca...  11.9 us
    scatter x1, local copies, waits for them, and re-layouts, shards(): slot_table = jnp.full((experts, capacity), tok_count, jnp.int32).at[flat_...  11.2 us
    scatter x1, local copies, waits for them, and re-layouts, shards(): weight_table = jnp.zeros((experts, capacity), jnp.float32).at[flat_routes...  11.2 us
    all_to_all x1, blocking collectives, shards(): lax.all_to_all(weight_table.astype(jnp.bfloat16), 'ep', split_axis=0, con...  9.88 us
  transfers between devices with their start and end apart: 5, of which 3 were waited for; matrix products, arithmetic and copies ran while one was open for 14% of the time, Pallas kernels for 0%

commit v1 on v0

v1 whole, which is shorter than its diff:
```python
import functools

import jax
import jax.numpy as jnp
from jax import lax
from jax.experimental import pallas as pl
from jax.experimental.pallas import tpu as pltpu
from jax.sharding import PartitionSpec as P

MESH = pl.DeviceIdType.MESH
BF16 = jnp.bfloat16
F32 = jnp.float32


def dispatch_kernel(
    dims,
    tok_ref,
    meta_ref,
    cot_ref,
    sh_ref,
    xfull,
    gfull,
    meta_out,
    cot_all,
    sh_out,
    local_sem,
    meta_send,
    meta_recv,
    tok_send,
    tok_recv,
    sh_send,
    sh_recv,
    cot_up,
    cot_down,
    cot_side,
    cot_recv,
    y_send,
    y_recv,
    sib_send,
    sib_recv,
):
    E, T, X, C, F, N = dims
    Y = T // 2
    NZ = E // X
    me = lax.axis_index("ep")
    tp = lax.axis_index("tp")
    y = tp // 2
    c = tp % 2
    sib = y * 2 + (1 - c)
    z = me // X
    x = me % X
    full = (xfull, gfull)

    barrier = pltpu.get_barrier_semaphore()

    def greet(d, _):
        pl.semaphore_signal(
            barrier, inc=1, device_id=((me + d) % E, tp), device_id_type=MESH
        )
        return 0

    lax.fori_loop(1, E, greet, 0)
    for dy in range(1, Y):
        pl.semaphore_signal(
            barrier, inc=1, device_id=(me, ((y + dy) % Y) * 2 + c), device_id_type=MESH
        )
    pl.semaphore_signal(barrier, inc=1, device_id=(me, sib), device_id_type=MESH)
    pl.semaphore_wait(barrier, (E - 1) + (Y - 1) + 1)

    def rows_of(s):
        return pl.ds(pl.multiple_of(s * C, 16), C)

    def cols_of(t):
        return pl.ds(pl.multiple_of(t * F, 128), F)

    def lanes_of(s):
        return pl.ds(pl.multiple_of(s * N, 128), N)

    def remote(src, dst, ss, rs, dev):
        return pltpu.make_async_remote_copy(
            src_ref=src,
            dst_ref=dst,
            send_sem=ss,
            recv_sem=rs,
            device_id=dev,
            device_id_type=MESH,
        )

    def meta_copy(dst):
        return remote(
            meta_ref.at[dst], meta_out.at[me], meta_send.at[dst], meta_recv.at[me], (dst, tp)
        )

    def tok_copy(dst):
        return remote(
            tok_ref.at[dst],
            xfull.at[rows_of(me), cols_of(tp)],
            tok_send.at[dst],
            tok_recv.at[me],
            (dst, tp),
        )

    def sh_copy(dst):
        return remote(
            sh_ref.at[dst], sh_out.at[:, lanes_of(me)], sh_send.at[dst], sh_recv.at[me], (dst, tp)
        )

    def cot_copy(s, sems, dst):
        return remote(cot_all.at[s], cot_all.at[s], sems.at[s], cot_recv.at[s], (dst, tp))

    locals_ = (
        pltpu.make_async_copy(cot_ref, cot_all.at[me], local_sem.at[0]),
        pltpu.make_async_copy(
            tok_ref.at[me], xfull.at[rows_of(me), cols_of(tp)], local_sem.at[1]
        ),
        pltpu.make_async_copy(meta_ref.at[me], meta_out.at[me], local_sem.at[2]),
        pltpu.make_async_copy(sh_ref.at[me], sh_out.at[:, lanes_of(me)], local_sem.at[3]),
    )
    for cp in locals_:
        cp.start()
    for cp in locals_:
        cp.wait()

    def each_source(fn, first=0):
        def step(i, _):
            k = i // X
            dz = ((k + 1) // 2) * (1 - 2 * (k % 2))
            zs = z + dz
            dx = i % X

            @pl.when((zs >= 0) & (zs < NZ))
            def _():
                fn(i, dz, dx, zs * X + (x + dx) % X)

            return 0

        lax.fori_loop(first, (2 * NZ - 1) * X, step, 0)

    def spread_cot(dz, s, act):
        @pl.when((dz <= 0) & (z + 1 < NZ))
        def _():
            act(cot_copy(s, cot_up, me + X))

        @pl.when((dz >= 0) & (z >= 1))
        def _():
            act(cot_copy(s, cot_down, me - X))

        for d in range(1, X):
            act(cot_copy(s, cot_side.at[d - 1], z * X + (x + d) % X))

    def start(cp):
        cp.start()

    def wait_send(cp):
        cp.wait_send()

    spread_cot(me * 0, me, start)

    def send_small(i, dz, dx, s):
        meta_copy(s).start()

    def send_rows(i, dz, dx, s):
        tok_copy(s).start()

    def send_shared(i, dz, dx, s):
        sh_copy(s).start()

    each_source(send_small, 1)
    each_source(send_rows, 1)
    each_source(send_shared, 1)

    def y_copy(a, s, dy):
        part = full[a].at[rows_of(s), cols_of(tp)]
        return remote(
            part,
            part,
            y_send.at[a, dy - 1],
            y_recv.at[a, dy - 1, s],
            (me, ((y + dy) % Y) * 2 + c),
        )

    def sib_copy(a, s, dy):
        part = full[a].at[rows_of(s), cols_of(((y + Y - dy) % Y) * 2 + c)]
        return remote(part, part, sib_send.at[a, dy], sib_recv.at[a, dy], (me, sib))

    def take(i, dz, dx, s):
        @pl.when(s != me)
        def _():
            remote(
                cot_all.at[s], cot_all.at[s], cot_up.at[s], cot_recv.at[s], (me, tp)
            ).wait_recv()

            @pl.when(dx == 0)
            def _():
                spread_cot(dz, s, start)

            remote(
                meta_ref.at[s], meta_out.at[s], meta_send.at[s], meta_recv.at[s], (me, tp)
            ).wait_recv()

        picked = jnp.dot(
            meta_out[s, :, :N], cot_all[s], preferred_element_type=F32
        ).astype(BF16)
        gfull[rows_of(s), cols_of(tp)] = picked

        @pl.when(s != me)
        def _():
            remote(
                tok_ref.at[s],
                xfull.at[rows_of(s), cols_of(tp)],
                tok_send.at[s],
                tok_recv.at[s],
                (me, tp),
            ).wait_recv()

        for a in (0, 1):
            for dy in range(1, Y):
                y_copy(a, s, dy).start()
            sib_copy(a, s, 0).start()

    def relay(i, dz, dx, s):
        for a in (0, 1):
            for dy in range(1, Y):
                part = full[a].at[rows_of(s), cols_of(((y + Y - dy) % Y) * 2 + c)]
                remote(
                    part, part, y_send.at[a, dy - 1], y_recv.at[a, dy - 1, s], (me, tp)
                ).wait_recv()
                sib_copy(a, s, dy).start()

    def guarded(fn, j):
        k = j // X
        dz = ((k + 1) // 2) * (1 - 2 * (k % 2))
        zs = z + dz
        dx = j % X

        @pl.when((j >= 0) & (zs >= 0) & (zs < NZ))
        def _():
            fn(j, dz, dx, zs * X + (x + dx) % X)

    total = (2 * NZ - 1) * X

    def main(i, _):
        guarded(take, i)
        guarded(relay, i - X)
        return 0

    lax.fori_loop(0, total, main, 0)
    for j in range(total - X, total):
        guarded(relay, jnp.int32(j))

    def finish(i, dz, dx, s):
        @pl.when(s != me)
        def _():
            meta_copy(s).wait_send()
            tok_copy(s).wait_send()
            sh_copy(s).wait_send()
            remote(
                sh_ref.at[s], sh_out.at[:, lanes_of(s)], sh_send.at[s], sh_recv.at[s], (me, tp)
            ).wait_recv()

        @pl.when(dx == 0)
        def _():
            spread_cot(dz, s, wait_send)

    each_source(finish)
    for a in (0, 1):
        mine = full[a].at[:, cols_of(tp)]
        for dy in range(1, Y):
            remote(mine, mine, y_send.at[a, dy - 1], y_send.at[a, dy - 1], (me, sib)).wait_send()
        for dy in range(Y):
            other = full[a].at[:, cols_of(((y + Y - dy) % Y) * 2 + 1 - c)]
            cp = remote(other, other, sib_send.at[a, dy], sib_recv.at[a, dy], (me, sib))
            cp.wait_send()
            cp.wait_recv()


def dispatch(E, T, C, F, N, rows, meta, cotangent, shared):
    X = 2 if E % 2 == 0 else 1
    Y = T // 2
    S = shared.shape[1]
    M = meta.shape[2]
    dma = pltpu.SemaphoreType.DMA
    vmem = pl.BlockSpec(memory_space=pltpu.VMEM)
    return pl.pallas_call(
        functools.partial(dispatch_kernel, (E, T, X, C, F, N)),
        out_shape=(
            jax.ShapeDtypeStruct((E * C, T * F), BF16),
            jax.ShapeDtypeStruct((E * C, T * F), BF16),
            jax.ShapeDtypeStruct((E, C, M), BF16),
            jax.ShapeDtypeStruct((E, N, F), BF16),
            jax.ShapeDtypeStruct((S, E * N), BF16),
        ),
        in_specs=[vmem] * 4,
        out_specs=(vmem,) * 5,
        scratch_shapes=[
            dma((4,)),
            dma((E,)),
            dma((E,)),
            dma((E,)),
            dma((E,)),
            dma((E,)),
            dma((E,)),
            dma((E,)),
            dma((E,)),
            dma((max(X - 1, 1), E)),
            dma((E,)),
            dma((2, max(Y - 1, 1))),
            dma((2, max(Y - 1, 1), E)),
            dma((2, Y)),
            dma((2, Y)),
        ],
        compiler_params=pltpu.CompilerParams(
            collective_id=0, has_side_effects=True, vmem_limit_bytes=48 * 1024 * 1024
        ),
        name="dispatch",
    )(rows, meta, cotangent, shared)


def shards(tokens, cotangent, routes, gate_weight, w_gate, w_up, w_down, shared_hidden):
    tok_count, top_count = routes.shape
    E = lax.axis_size("ep")
    T = lax.axis_size("tp")
    F = tokens.shape[1]
    capacity = 3 * tok_count * top_count // (2 * E)
    C = -(-capacity // 16) * 16
    R = E * C
    flat_routes = routes.reshape(-1)
    onehot = (flat_routes[:, None] == jnp.arange(E, dtype=jnp.int32)[None, :]).astype(F32)
    count = tok_count * top_count
    before = (
        jnp.arange(count, dtype=jnp.int32)[:, None] > jnp.arange(count, dtype=jnp.int32)[None, :]
    ).astype(BF16)
    earlier = jnp.dot(before, onehot.astype(BF16), preferred_element_type=F32)
    positions = jnp.sum(earlier * onehot, axis=1).astype(jnp.int32)
    slots = (flat_routes * C + positions).reshape(tok_count, top_count)
    lines = jnp.arange(R, dtype=jnp.int32)[:, None]
    masks = [slots[:, k][None, :] == lines for k in range(top_count)]
    select = functools.reduce(jnp.logical_or, masks).astype(BF16)
    weight = sum(
        jnp.sum(jnp.where(m, gate_weight[:, k][None, :], 0.0), axis=1)
        for k, m in enumerate(masks)
    )
    high = lax.reduce_precision(weight, 8, 7)
    low = weight - high
    tail = jnp.arange(128, dtype=jnp.int32)[None, :]
    extra = jnp.where(
        tail == 0, high[:, None], jnp.where(tail == 1, low[:, None], 0.0)
    ).astype(BF16)
    meta = jnp.concatenate([select, extra], axis=1).reshape(E, C, tok_count + 128)
    rows = jnp.dot(select, tokens, preferred_element_type=F32).astype(BF16).reshape(E, C, F)
    shared = shared_hidden.T.reshape(E, shared_hidden.shape[1] // E, tok_count)

    rows_x, rows_g, meta_got, cot_all, shared_got = dispatch(
        E, T, C, F, tok_count, rows, meta, cotangent, shared
    )
    got = meta_got.reshape(R, tok_count + 128)
    weight_col = got[:, tok_count : tok_count + 1].astype(F32) + got[
        :, tok_count + 1 : tok_count + 2
    ].astype(F32)
    contract_last = (((1,), (1,)), ((), ()))
    gate_mat = w_gate[0]
    up_mat = w_up[0]
    down_mat = w_down[0]
    pre_gate = lax.dot_general(rows_x, gate_mat, contract_last, preferred_element_type=F32)
    pre_up = lax.dot_general(rows_x, up_mat, contract_last, preferred_element_type=F32)
    sigmoid_gate = jax.nn.sigmoid(pre_gate)
    silu_gate = pre_gate * sigmoid_gate
    hidden = (silu_gate * pre_up).astype(BF16)
    back_hidden = lax.dot_general(rows_g, down_mat, contract_last, preferred_element_type=F32)
    gate_part = jnp.sum(hidden.astype(F32) * back_hidden, axis=1)
    scaled = weight_col * back_hidden
    grad_pre_gate = (
        scaled * pre_up * sigmoid_gate * (1.0 + pre_gate * (1.0 - sigmoid_gate))
    ).astype(BF16)
    grad_pre_up = (scaled * silu_gate).astype(BF16)
    weighted_cotan = (weight_col * rows_g.astype(F32)).astype(BF16)
    grad_down = jnp.dot(hidden.T, weighted_cotan, preferred_element_type=F32)
    grad_gate = jnp.dot(grad_pre_gate.T, rows_x, preferred_element_type=F32)
    grad_up = jnp.dot(grad_pre_up.T, rows_x, preferred_element_type=F32)
    partial_value = jnp.dot(grad_pre_gate, gate_mat, preferred_element_type=F32)
    partial_value = partial_value + jnp.dot(grad_pre_up, up_mat, preferred_element_type=F32)
    shared_grad = jnp.dot(
        shared_got, cot_all.reshape(E * tok_count, F), preferred_element_type=F32
    )
    row_share = lax.psum_scatter(
        partial_value.astype(BF16).reshape(E, C, T * F), "tp", scatter_dimension=2, tiled=True
    )
    gate_total = lax.psum(gate_part.reshape(E, C), "tp")
    back_rows = lax.all_to_all(row_share, "ep", split_axis=0, concat_axis=0, tiled=True)
    back_gate = lax.all_to_all(
        gate_total.astype(BF16), "ep", split_axis=0, concat_axis=0, tiled=True
    ).astype(F32)
    tokens_grad = lax.dot_general(
        select, back_rows.reshape(R, F), (((0,), (0,)), ((), ())), preferred_element_type=F32
    ).astype(BF16)
    gate_grad = jnp.stack(
        [jnp.sum(jnp.where(m, back_gate.reshape(R, 1), 0.0), axis=0) for m in masks], axis=1
    )
    return (tokens_grad, gate_grad, grad_gate[None], grad_up[None], grad_down[None], shared_grad)


def solution(mesh):
    placed = (
        P("ep", "tp"),
        P("ep", "tp"),
        P("ep", None),
        P("ep", None),
        P("ep", "tp", None),
        P("ep", "tp", None),
        P("ep", "tp", None),
        P("ep", None),
    )
    return jax.shard_map(
        shards,
        mesh=mesh,
        in_specs=placed,
        out_specs=(
            P("ep", "tp"),
            P("ep", None),
            P("ep", "tp", None),
            P("ep", "tp", None),
            P("ep", "tp", None),
            P("ep", "tp"),
        ),
        check_vma=False,
    )
```

time: 264 us -> 169 us (0.64)
  waiting for transfers between devices: 96.6 us -> 23.5 us
  Pallas kernels: 0 us -> 69 us
  blocking collectives: 78.3 us -> 16.8 us
  local copies, waits for them, and re-layouts: 36.4 us -> 5.22 us
  matrix products: 27.7 us -> 32.3 us
  other arithmetic: 4.71 us -> 2.02 us
    reduce_scatter x2 -> x1, waiting for transfers between devices: 91.3 us -> 19.1 us  [shards(): lax.psum_scatter(partial_value.astype(BF16).reshape(E, C, T * F), 'tp', s...]
    pallas_call x0 -> x1, Pallas kernels: none -> 69 us  [dispatch(): pl.pallas_call(functools.partial(dispatch_kernel, (E, T, X, C, F, N)), ou...]
    all_to_all x4 -> x1, blocking collectives: 72.4 us -> 8.85 us  [shards(): lax.all_to_all(gate_total.astype(BF16), 'ep', split_axis=0, concat_axis=0...]
    scatter x2 -> x0, local copies, waits for them, and re-layouts: 22.4 us -> none  [the longest x1 11.2 us: shards(): slot_table = jnp.full((experts, capacity), tok_count, jnp.int32).at[flat_...]
    gather x5 -> x0, local copies, waits for them, and re-layouts: 8.51 us -> none  [the longest x2 4.14 us: place_rows(): return padded[slot_table]]
    all_gather x2 -> x0, waiting for transfers between devices: 5.23 us -> none  [the longest x1 5.22 us: shards(): lax.all_gather(part_cotan, 'tp', axis=2, tiled=True)]
    dot_general x9 -> x12, matrix products: 27.7 us -> 32.3 us  [the longest x1 5.31 us: shards(): grad_gate = jnp.dot(grad_pre_gate.T, rows_x, preferred_element_type=F32)]
    all_to_all x1, waiting for transfers between devices: 0.01 us -> 4.42 us  [shards(): lax.all_to_all(row_share, 'ep', split_axis=0, concat_axis=0, tiled=True)]
  transfers between devices with their start and end apart: 5 -> 2, of which waited for: 3 -> 2; matrix products, arithmetic and copies ran while one was open for 14% -> 9% of each run, Pallas kernels for 0% -> 0%
where the time goes in v1:
time: 169 us
  Pallas kernels  69 us (41%)
  matrix products  32.3 us (19%)
  waiting for transfers between devices  23.5 us (14%)
  blocking collectives  16.8 us (10%)
  between operations  14.2 us (8%)
  starting transfers between devices  5.55 us (3%)
  local copies, waits for them, and re-layouts  5.22 us (3%)
  other arithmetic  2.02 us (1%)
    pallas_call x1, Pallas kernels, dispatch(): pl.pallas_call(functools.partial(dispatch_kernel, (E, T, X, C, F, N)), ou...  69 us
    reduce_scatter x1, waiting for transfers between devices, shards(): lax.psum_scatter(partial_value.astype(BF16).reshape(E, C, T * F), 'tp', s...  19.1 us
    all_to_all x1, blocking collectives, shards(): lax.all_to_all(gate_total.astype(BF16), 'ep', split_axis=0, concat_axis=0...  8.85 us
    psum x1, blocking collectives, shards(): gate_total = lax.psum(gate_part.reshape(E, C), 'tp')  7.95 us
    all_to_all x1, starting transfers between devices, shards(): lax.all_to_all(row_share, 'ep', split_axis=0, concat_axis=0, tiled=True)  5.51 us
    dot_general x1, matrix products, shards(): grad_gate = jnp.dot(grad_pre_gate.T, rows_x, preferred_element_type=F32)  5.31 us
    dot_general x1, matrix products, shards(): lax.dot_general(rows_g, down_mat, contract_last, preferred_element_type=F32)  4.6 us
    dot_general x1, matrix products, shards(): lax.dot_general(rows_x, up_mat, contract_last, preferred_element_type=F32)  4.6 us
  transfers between devices with their start and end apart: 2, of which 2 were waited for; matrix products, arithmetic and copies ran while one was open for 9% of the time, Pallas kernels for 0%

profile of v1, /device:TPU:0, one launch (start us, length us, event | category | flops | bytes accessed | tf_op | source)
XLA Modules:
  0.0 168.7 jit_solution(1657349774583051405)
XLA Ops:
  7.2 0.0 copy-start
  7.2 0.0 reduce-scatter.2.cloned.1.call-start
  7.3 0.9 copy.47
  8.2 0.1 eq.91
  8.3 0.2 fusion.10
  8.5 0.1 convert_element_type.71
  8.7 0.1 copy.48
  8.7 0.7 multiply_add_fusion.1
  9.4 0.8 slice_bitcast_fusion
  10.2 1.3 convolution_convert_fusion
  11.5 0.2 select_reduce_fusion.2
  11.7 0.1 add.40
  11.8 0.1 or_convert_fusion
  11.9 1.1 copy.49
  13.1 0.2 select_convert_fusion
  13.3 0.0 copy-start.2
  13.3 0.9 copy-done.2
  14.2 69.0 %dispatch.1 = (bf16[384,4096]{1,0:T(8,128)(2,1)}, bf16[384,4096]{1,0:T(8,128)(2,1)}, bf16[8,48,256]{2,1,0:T(8,128)(2,1)S(1)}, bf16[8,128,1024]{2,1,0:T(8,128)(2,1)S(1)}, bf16[128,1024]{1,0:T(8,128)(2,1)S(1)}) custom-call(bf16[8,48,1024]{2,1,0:T(8,128)(2,1)S(1)} %bitcast.55, bf16[8,48,256]{2,1,0:T(8,128)(2,1)S(1)} %pad_maximum_fusion.meta_ref, ...), custom_call_target="tpu_custom_call" | custom-call | tf_op jit(solution)/shard_map/dispatch/pallas_call | solution.py:284
  83.2 0.0 copy-start.1
  83.3 0.0 copy-start.3
  83.3 4.6 %fusion.6 = f32[384,256]{0,1:T(8,128)S(1)} fusion(bf16[384,4096]{1,0:T(8,128)(2,1)} %get-tuple-element.13, bf16[1,256,4096]{2,1,0:T(8,128)(2,1)} %param.13), kind=kOutput, calls=%fused_computation.11 | convolution fusion | flops 805306368 | bytes 5636096 | tf_op jit(solution)/shard_map/dot_general | solution.py:365
  87.9 0.0 copy-done
  87.9 0.0 copy-done.3
  87.9 2.0 %fusion.3 = f32[384,256]{0,1:T(8,128)} fusion(bf16[384,4096]{1,0:T(8,128)(2,1)S(1)} %copy-done.3, bf16[1,256,4096]{2,1,0:T(8,128)(2,1)S(1)} %copy-done), kind=kOutput, calls=%fused_computation.8 | convolution fusion | flops 805306368 | bytes 5636096 | tf_op jit(solution)/shard_map/dot_general | solution.py:364
  89.9 0.0 copy-done.1
  89.9 0.1 fusion.20
  90.0 0.1 copy.54
  90.1 0.1 copy.53
  90.2 4.6 %multiply_reduce_fusion = (f32[384]{0:T(512)S(1)}, bf16[384,256]{0,1:T(8,128)(2,1)}, bf16[384,256]{0,1:T(8,128)(2,1)S(1)}, bf16[384,256]{0,1:T(8,128)(2,1)S(1)}) fusion(f32[384,256]{0,1:T(8,128)S(1)} %fusion.6, f32[384,256]{0,1:T(8,128)} %fusion.3, f32[384]{0:T(512)S(1)} %add_reduce_fusion, bf16[384,4096]{1,0:T(8,128)(2,1)} %get-tuple-element.12, ...), kind=kOutput, calls=%fused_computation.19 | convolution fusion | flops 807173760 | bytes 6622208 | tf_op jit(solution)/shard_map/dot_general | solution.py:369
  94.9 0.0 copy-start.6
  94.9 1.0 fusion.1
  95.9 0.6 copy-done.6
  96.4 2.7 %add_convert_fusion = bf16[384,4096]{1,0:T(8,128)(2,1)} fusion(f32[384,4096]{1,0:T(8,128)S(1)} %fusion.1, bf16[384,256]{0,1:T(8,128)(2,1)S(1)} %get-tuple-element.21, bf16[1,256,4096]{2,1,0:T(8,128)(2,1)S(1)} %copy-done.6), kind=kOutput, calls=%fused_computation.1 | convolution fusion | flops 808452096 | bytes 11730944 | tf_op jit(solution)/shard_map/dot_general | solution.py:381
  99.1 0.0 reduce-scatter.2.cloned.1.call-update
  99.2 0.1 reshape.129
  99.2 8.0 %psum.7 = bf16[8,48]{1,0:T(8,128)(2,1)S(1)} all-reduce(f32[8,48]{1,0:T(8,128)S(1)} %reshape.129), channel_id=1, replica_groups=mesh['ep'=8,'tp'=4] {'tp'}, use_global_device_ids=true, to_apply=%region_5.6 | all-reduce | flops 384 | bytes 2304 | tf_op jit(solution)/shard_map/psum | solution.py:388
  107.2 8.8 %all_to_all.14 = bf16[8,1,48]{2,1,0:T(2,128)(2,1)S(1)} all-to-all(bf16[8,1,48]{2,1,0:T(2,128)(2,1)S(1)} %copy.52), channel_id=1, replica_groups=mesh['ep'=8,'tp'=4] {'ep'}, dimensions={0} | all-to-all | bytes 1536 | tf_op jit(solution)/shard_map/all_to_all | solution.py:390
  116.0 19.1 %reduce-scatter.2.cloned.1.call-done = bf16[8,48,1024]{2,1,0:T(8,128)(2,1)} async-done(((bf16[8,48,4096]{2,1,0:T(8,128)(2,1)}), bf16[8,48,1024]{2,1,0:T(8,128)(2,1)}) %reduce-scatter.2.cloned.1.call-update) | async-done | bytes 786448 | tf_op jit(solution)/shard_map/reduce_scatter | solution.py:385
  135.2 5.5 %all-to-all-start = ((bf16[8,48,1024]{2,1,0:T(8,128)(2,1)}), bf16[8,48,1024]{2,1,0:T(8,128)(2,1)S(1)}, u32[]{:S(2)}, u32[]{:S(2)}) async-start(bf16[8,48,1024]{2,1,0:T(8,128)(2,1)} %reduce-scatter.2.cloned.1.call-done), calls=%async_computation.1 | async-start | bytes 1572864 | tf_op jit(solution)/shard_map/all_to_all | solution.py:389
  140.7 2.8 %fusion.22 = f32[128,1024]{1,0:T(8,128)} fusion(bf16[128,1024]{1,0:T(8,128)(2,1)S(1)} %get-tuple-element.14, bf16[1024,1024]{1,0:T(8,128)(2,1)} %bitcast.56), kind=kOutput, calls=%fused_computation.58 | convolution fusion | flops 268435456 | bytes 2883584 | tf_op jit(solution)/shard_map/dot_general | solution.py:382
  143.5 0.0 copy-start.4
  143.5 5.3 %convolution_bitcast_fusion.2 = f32[1,256,4096]{2,1,0:T(8,128)} fusion(bf16[384,256]{0,1:T(8,128)(2,1)S(1)} %get-tuple-element.20, bf16[384,4096]{1,0:T(8,128)(2,1)} %get-tuple-element.13), kind=kOutput, calls=%fused_computation.4 | convolution fusion | flops 805306368 | bytes 7536640 | tf_op jit(solution)/shard_map/dot_general | solution.py:378
  148.8 0.0 copy-done.4
  148.8 0.0 copy-start.5
  148.8 0.0 copy-start.7
  148.8 3.3 %convolution_bitcast_fusion.1 = f32[1,256,4096]{2,1,0:T(8,128)} fusion(bf16[384,256]{0,1:T(8,128)(2,1)S(1)} %get-tuple-element.21, bf16[384,4096]{1,0:T(8,128)(2,1)S(1)} %copy-done.4), kind=kOutput, calls=%fused_computation.3 | convolution fusion | flops 805306368 | bytes 7536640 | tf_op jit(solution)/shard_map/dot_general | solution.py:379
  152.1 0.0 copy-done.5
  152.1 0.0 copy-done.7
  152.1 3.4 %convolution_bitcast_fusion = f32[1,256,4096]{2,1,0:T(8,128)} fusion(bf16[384,256]{0,1:T(8,128)(2,1)S(1)} %copy-done.7, bf16[384,4096]{1,0:T(8,128)(2,1)S(1)} %copy-done.5, f32[384]{0:T(512)S(1)} %add_reduce_fusion), kind=kOutput, calls=%fused_computation.2 | convolution fusion | flops 810024960 | bytes 7538176 | tf_op jit(solution)/shard_map/dot_general | solution.py:377
  155.5 0.1 reshape.131
  155.6 0.1 select_reduce_fusion.1
  155.8 0.6 pad_maximum_fusion.1
  156.3 4.4 %all-to-all-done = bf16[8,48,1024]{2,1,0:T(8,128)(2,1)S(1)} async-done(((bf16[8,48,1024]{2,1,0:T(8,128)(2,1)}), bf16[8,48,1024]{2,1,0:T(8,128)(2,1)S(1)}, u32[]{:S(2)}, u32[]{:S(2)}) %all-to-all-start) | async-done | bytes 786464 | tf_op jit(solution)/shard_map/all_to_all | solution.py:389
  160.8 1.1 convolution_convert_fusion.1
  (10 shorter events, 0.1 us)
Async XLA Ops:
  7.2 80.7 %copy-start = (bf16[1,256,4096]{2,1,0:T(8,128)(2,1)S(1)}, bf16[1,256,4096]{2,1,0:T(8,128)(2,1)}, u32[]{:S(2)}) copy-start(bf16[1,256,4096]{2,1,0:T(8,128)(2,1)} %param.12) | copy-start | bytes 6291460
  7.2 128.0 %reduce-scatter.2.cloned.1.call-start = ((), (), s32[]{:S(2)}) async-start(), calls=%async_computation.3 | async-start | bytes 3932160 | tf_op jit(solution)/shard_map/reduce_scatter | solution.py:385
  13.3 1.0 copy-start.2
  83.2 6.7 %copy-start.1 = (bf16[8,128,1024]{2,1,0:T(8,128)(2,1)}, bf16[8,128,1024]{2,1,0:T(8,128)(2,1)S(1)}, u32[]{:S(2)}) copy-start(bf16[8,128,1024]{2,1,0:T(8,128)(2,1)S(1)} %get-tuple-element.15) | copy-start | bytes 6291460
  83.3 4.6 %copy-start.3 = (bf16[384,4096]{1,0:T(8,128)(2,1)S(1)}, bf16[384,4096]{1,0:T(8,128)(2,1)}, u32[]{:S(2)}) copy-start(bf16[384,4096]{1,0:T(8,128)(2,1)} %get-tuple-element.13) | copy-start | bytes 9437188
  94.9 1.6 copy-start.6
  135.2 25.6 %all-to-all-start = ((bf16[8,48,1024]{2,1,0:T(8,128)(2,1)}), bf16[8,48,1024]{2,1,0:T(8,128)(2,1)S(1)}, u32[]{:S(2)}, u32[]{:S(2)}) async-start(bf16[8,48,1024]{2,1,0:T(8,128)(2,1)} %reduce-scatter.2.cloned.1.call-done), calls=%async_computation.1 | async-start | bytes 1572864 | tf_op jit(solution)/shard_map/all_to_all | solution.py:389
  143.5 5.3 %copy-start.4 = (bf16[384,4096]{1,0:T(8,128)(2,1)S(1)}, bf16[384,4096]{1,0:T(8,128)(2,1)}, u32[]{:S(2)}) copy-start(bf16[384,4096]{1,0:T(8,128)(2,1)} %get-tuple-element.13) | copy-start | bytes 9437188
  148.8 3.3 %copy-start.5 = (bf16[384,4096]{1,0:T(8,128)(2,1)S(1)}, bf16[384,4096]{1,0:T(8,128)(2,1)}, u32[]{:S(2)}) copy-start(bf16[384,4096]{1,0:T(8,128)(2,1)} %get-tuple-element.12) | copy-start | bytes 9437188
  148.8 3.3 %copy-start.7 = (bf16[384,256]{0,1:T(8,128)(2,1)S(1)}, bf16[384,256]{0,1:T(8,128)(2,1)}, u32[]{:S(2)}) copy-start(bf16[384,256]{0,1:T(8,128)(2,1)} %get-tuple-element.19) | copy-start | bytes 589828
Sparse Core Ops, SparseCore 0:
  99.3 35.8 reduce-scatter.1

commit v2 on v1

--- a/solution.py
+++ b/solution.py
@@ -162,12 +162,8 @@
     def send_rows(i, dz, dx, s):
         tok_copy(s).start()
 
-    def send_shared(i, dz, dx, s):
-        sh_copy(s).start()
-
     each_source(send_small, 1)
     each_source(send_rows, 1)
-    each_source(send_shared, 1)
 
     def y_copy(a, s, dy):
         part = full[a].at[rows_of(s), cols_of(tp)]
@@ -183,26 +179,12 @@
         part = full[a].at[rows_of(s), cols_of(((y + Y - dy) % Y) * 2 + c)]
         return remote(part, part, sib_send.at[a, dy], sib_recv.at[a, dy], (me, sib))
 
-    def take(i, dz, dx, s):
-        @pl.when(s != me)
-        def _():
-            remote(
-                cot_all.at[s], cot_all.at[s], cot_up.at[s], cot_recv.at[s], (me, tp)
-            ).wait_recv()
-
-            @pl.when(dx == 0)
-            def _():
-                spread_cot(dz, s, start)
-
-            remote(
-                meta_ref.at[s], meta_out.at[s], meta_send.at[s], meta_recv.at[s], (me, tp)
-            ).wait_recv()
-
-        picked = jnp.dot(
-            meta_out[s, :, :N], cot_all[s], preferred_element_type=F32
-        ).astype(BF16)
-        gfull[rows_of(s), cols_of(tp)] = picked
-
+    def forward(a, s):
+        for dy in range(1, Y):
+            y_copy(a, s, dy).start()
+        sib_copy(a, s, 0).start()
+
+    def take_rows(i, dz, dx, s):
         @pl.when(s != me)
         def _():
             remote(
@@ -213,19 +195,46 @@
                 (me, tp),
             ).wait_recv()
 
-        for a in (0, 1):
-            for dy in range(1, Y):
-                y_copy(a, s, dy).start()
-            sib_copy(a, s, 0).start()
-
-    def relay(i, dz, dx, s):
-        for a in (0, 1):
-            for dy in range(1, Y):
-                part = full[a].at[rows_of(s), cols_of(((y + Y - dy) % Y) * 2 + c)]
-                remote(
-                    part, part, y_send.at[a, dy - 1], y_recv.at[a, dy - 1, s], (me, tp)
-                ).wait_recv()
-                sib_copy(a, s, dy).start()
+        forward(0, s)
+
+    def take_cot(i, dz, dx, s):
+        @pl.when(s != me)
+        def _():
+            remote(
+                cot_all.at[s], cot_all.at[s], cot_up.at[s], cot_recv.at[s], (me, tp)
+            ).wait_recv()
+
+            @pl.when(dx == 0)
+            def _():
+                spread_cot(dz, s, start)
+
+            remote(
+                meta_ref.at[s], meta_out.at[s], meta_send.at[s], meta_recv.at[s], (me, tp)
+            ).wait_recv()
+
+        picked = jnp.dot(
+            meta_out[s, :, :N], cot_all[s], preferred_element_type=F32
+        ).astype(BF16)
+        gfull[rows_of(s), cols_of(tp)] = picked
+        forward(1, s)
+
+        @pl.when(s != me)
+        def _():
+            sh_copy(s).start()
+
+    def relay(a, s):
+        for dy in range(1, Y):
+            part = full[a].at[rows_of(s), cols_of(((y + Y - dy) % Y) * 2 + c)]
+            remote(
+                part, part, y_send.at[a, dy - 1], y_recv.at[a, dy - 1, s], (me, tp)
+            ).wait_recv()
+            sib_copy(a, s, dy).start()
+
+    def relay_rows(i, dz, dx, s):
+        relay(0, s)
+
+    def relay_cot(i, dz, dx, s):
+        relay(1, s)
 
     def guarded(fn, j):
         k = j // X
@@ -240,13 +249,13 @@
     total = (2 * NZ - 1) * X
 
     def main(i, _):
-        guarded(take, i)
-        guarded(relay, i - X)
+        guarded(take_rows, i)
+        guarded(take_cot, i - X)
+        guarded(relay_rows, i - X)
+        guarded(relay_cot, i - 2 * X)
         return 0
 
-    lax.fori_loop(0, total, main, 0)
-    for j in range(total - X, total):
-        guarded(relay, jnp.int32(j))
+    lax.fori_loop(0, total + 2 * X, main, 0)
 
     def finish(i, dz, dx, s):
         @pl.when(s != me)
@@ -314,6 +323,217 @@
         ),
         name="dispatch",
     )(rows, meta, cotangent, shared)
+
+
+def return_kernel(
+    dims,
+    part,
+    gate,
+    back,
+    gate_back,
+    pair_in,
+    y_out,
+    y_in,
+    row_out,
+    gate_in,
+    gate_out,
+    pair_send,
+    pair_recv,
+    y_send,
+    y_recv,
+    back_send,
+    back_recv,
+    gate_tp_send,
+    gate_tp_recv,
+    gate_ep_send,
+    gate_ep_recv,
+):
+    E, T, C, F = dims
+    Y = T // 2
+    me = lax.axis_index("ep")
+    tp = lax.axis_index("tp")
+    y = tp // 2
+    c = tp % 2
+    sib = y * 2 + (1 - c)
+
+    barrier = pltpu.get_barrier_semaphore()
+
+    def greet(d, _):
+        pl.semaphore_signal(
+            barrier, inc=1, device_id=((me + d) % E, tp), device_id_type=MESH
+        )
+        return 0
+
+    lax.fori_loop(1, E, greet, 0)
+    for dt in range(1, T):
+        pl.semaphore_signal(
+            barrier, inc=1, device_id=(me, (tp + dt) % T), device_id_type=MESH
+        )
+    pl.semaphore_wait(barrier, (E - 1) + (T - 1))
+
+    def rows_of(s):
+        return pl.ds(pl.multiple_of(s * C, 16), C)
+
+    def cols_of(t):
+        return pl.ds(pl.multiple_of(t * F, 128), F)
+
+    def remote(src, dst, ss, rs, dev):
+        return pltpu.make_async_remote_copy(
+            src_ref=src,
+            dst_ref=dst,
+            send_sem=ss,
+            recv_sem=rs,
+            device_id=dev,
+            device_id_type=MESH,
+        )
+
+    def source(i):
+        return (me + E // 2 + i) % E
+
+    def pair_copy(s, dy):
+        return remote(
+            part.at[rows_of(s), cols_of(((y + dy) % Y) * 2 + 1 - c)],
+            pair_in.at[dy, rows_of(s)],
+            pair_send.at[dy],
+            pair_recv.at[dy, s],
+            (me, sib),
+        )
+
+    def gate_tp_copy(dt):
+        return remote(
+            gate, gate_in.at[dt], gate_tp_send.at[dt], gate_tp_recv.at[dt], (me, (tp + dt) % T)
+        )
+
+    def gate_ep_copy(s):
+        return remote(gate_out.at[s], gate_back.at[me], gate_ep_send, gate_ep_recv, (s, tp))
+
+    def y_copy(s, dy):
+        return remote(
+            y_out.at[dy - 1, rows_of(s)],
+            y_in.at[dy - 1, rows_of(s)],
+            y_send.at[dy - 1],
+            y_recv.at[dy - 1, s],
+            (me, ((y + dy) % Y) * 2 + c),
+        )
+
+    def back_copy(s):
+        return remote(row_out.at[rows_of(s)], back.at[me], back_send, back_recv, (s, tp))
+
+    for dt in range(1, T):
+        gate_tp_copy(dt).start()
+
+    def open_pairs(i, _):
+        for dy in list(range(1, Y)) + [0]:
+            pair_copy(source(i), dy).start()
+        return 0
+
+    lax.fori_loop(0, E, open_pairs, 0)
+
+    def mix(s, dy):
+        pair_copy(s, dy).wait_recv()
+        return part[rows_of(s), cols_of(((y + dy) % Y) * 2 + c)].astype(F32) + pair_in[
+            dy, rows_of(s), :
+        ].astype(F32)
+
+    def cross(s):
+        for dy in range(1, Y):
+            y_out[dy - 1, rows_of(s), :] = mix(s, dy).astype(BF16)
+            y_copy(s, dy).start()
+
+    def send_back(s):
+        value = mix(s, 0)
+        for dy in range(1, Y):
+            y_copy(s, dy).wait_recv()
+            value = value + y_in[dy - 1, rows_of(s), :].astype(F32)
+        value = value.astype(BF16)
+
+        @pl.when(s != me)
+        def _():
+            row_out[rows_of(s), :] = value
+            back_copy(s).start()
+
+        @pl.when(s == me)
+        def _():
+            back[me] = value
+
+    def main(i, _):
+        @pl.when(i < E)
+        def _():
+            cross(source(i))
+
+        @pl.when(i >= 2)
+        def _():
+            send_back(source(i - 2))
+
+        return 0
+
+    lax.fori_loop(0, E + 2, main, 0)
+
+    total = gate[...]
+    for dt in range(1, T):
+        gate_tp_copy(dt).wait()
+        total = total + gate_in[dt]
+    gate_out[...] = total
+    gate_back[me] = gate_out[me]
+
+    def gates(d, _):
+        gate_ep_copy((me + d) % E).start()
+        return 0
+
+    lax.fori_loop(1, E, gates, 0)
+
+    for dy in range(Y):
+        everything = pair_in.at[dy]
+        remote(everything, everything, pair_send.at[dy], pair_send.at[dy], (me, sib)).wait_send()
+    for dy in range(1, Y):
+        everything = y_in.at[dy - 1]
+        remote(everything, everything, y_send.at[dy - 1], y_send.at[dy - 1], (me, sib)).wait_send()
+    blocks = back.at[pl.ds(0, E - 1)]
+    done = remote(blocks, blocks, back_send, back_recv, (me, sib))
+    done.wait_send()
+    done.wait_recv()
+    blocks = gate_back.at[pl.ds(0, E - 1)]
+    done = remote(blocks, blocks, gate_ep_send, gate_ep_recv, (me, sib))
+    done.wait_send()
+    done.wait_recv()
+
+
+def send_home(E, T, C, F, part, gate):
+    Y = T // 2
+    R = E * C
+    dma = pltpu.SemaphoreType.DMA
+    vmem = pl.BlockSpec(memory_space=pltpu.VMEM)
+    return pl.pallas_call(
+        functools.partial(return_kernel, (E, T, C, F)),
+        out_shape=(
+            jax.ShapeDtypeStruct((E, C, F), BF16),
+            jax.ShapeDtypeStruct(gate.shape, F32),
+        ),
+        in_specs=[vmem] * 2,
+        out_specs=(vmem,) * 2,
+        scratch_shapes=[
+            pltpu.VMEM((Y, R, F), BF16),
+            pltpu.VMEM((max(Y - 1, 1), R, F), BF16),
+            pltpu.VMEM((max(Y - 1, 1), R, F), BF16),
+            pltpu.VMEM((R, F), BF16),
+            pltpu.VMEM((T,) + gate.shape, F32),
+            pltpu.VMEM(gate.shape, F32),
+            dma((Y,)),
+            dma((Y, E)),
+            dma((max(Y - 1, 1),)),
+            dma((max(Y - 1, 1), E)),
+            dma,
+            dma,
+            dma((T,)),
+            dma((T,)),
+            dma,
+            dma,
+        ],
+        compiler_params=pltpu.CompilerParams(
+            collective_id=1, has_side_effects=True, vmem_limit_bytes=40 * 1024 * 1024
+        ),
+        name="send_home",
+    )(part, gate)
 
 
 def shards(tokens, cotangent, routes, gate_weight, w_gate, w_up, w_down, shared_hidden):
@@ -382,14 +602,9 @@
     shared_grad = jnp.dot(
         shared_got, cot_all.reshape(E * tok_count, F), preferred_element_type=F32
     )
-    row_share = lax.psum_scatter(
-        partial_value.astype(BF16).reshape(E, C, T * F), "tp", scatter_dimension=2, tiled=True
-    )
-    gate_total = lax.psum(gate_part.reshape(E, C), "tp")
-    back_rows = lax.all_to_all(row_share, "ep", split_axis=0, concat_axis=0, tiled=True)
-    back_gate = lax.all_to_all(
-        gate_total.astype(BF16), "ep", split_axis=0, concat_axis=0, tiled=True
-    ).astype(F32)
+    gate_box = jnp.pad(gate_part.reshape(E, 1, C), ((0, 0), (0, 7), (0, 128 - C)))
+    back_rows, back_gate = send_home(E, T, C, F, partial_value.astype(BF16), gate_box)
+    back_gate = back_gate[:, 0, :C]
     tokens_grad = lax.dot_general(
         select, back_rows.reshape(R, F), (((0,), (0,)), ((), ())), preferred_element_type=F32
     ).astype(BF16)

time: 169 us -> 138 us (0.82)
  Pallas kernels: 69 us -> 97.3 us
  waiting for transfers between devices: 23.5 us -> 0 us
  blocking collectives: 16.8 us -> 0 us
  between operations: 14.2 us -> 0.84 us
  starting transfers between devices: 5.55 us -> 0 us
  matrix products: 32.3 us -> 30.2 us
  local copies, waits for them, and re-layouts: 5.22 us -> 7.16 us
    pallas_call x0 -> x1, Pallas kernels: none -> 31.3 us  [send_home(): pl.pallas_call(functools.partial(return_kernel, (E, T, C, F)), out_shape=...]
    reduce_scatter x1 -> x0, waiting for transfers between devices: 19.1 us -> none  [shards(): lax.psum_scatter(partial_value.astype(BF16).reshape(E, C, T * F), 'tp', s...]
    all_to_all x1 -> x0, blocking collectives: 8.85 us -> none  [shards(): lax.all_to_all(gate_total.astype(BF16), 'ep', split_axis=0, concat_axis=0...]
    psum x1 -> x0, blocking collectives: 7.95 us -> none  [shards(): gate_total = lax.psum(gate_part.reshape(E, C), 'tp')]
    all_to_all x1 -> x0, starting transfers between devices: 5.51 us -> none  [shards(): lax.all_to_all(row_share, 'ep', split_axis=0, concat_axis=0, tiled=True)]
    all_to_all x1 -> x0, waiting for transfers between devices: 4.42 us -> none  [shards(): lax.all_to_all(row_share, 'ep', split_axis=0, concat_axis=0, tiled=True)]
    pallas_call x1, Pallas kernels: 69 us -> 66 us  [dispatch(): pl.pallas_call(functools.partial(dispatch_kernel, (E, T, X, C, F, N)), ou...]
    unnamed x19 -> x25, local copies, waits for them, and re-layouts: 2.67 us -> 4.57 us
  transfers between devices with their start and end apart: 2 -> 0, of which waited for: 2 -> 0; matrix products, arithmetic and copies ran while one was open for 9% -> 0% of each run, Pallas kernels for 0% -> 0%
where the time goes in v2:
time: 138 us; the launch traced here: 137 us
  Pallas kernels  97.3 us (71%)
  matrix products  30.2 us (22%)
  local copies, waits for them, and re-layouts  7.16 us (5%)
  other arithmetic  1.99 us (1%)
    pallas_call x1, Pallas kernels, dispatch(): pl.pallas_call(functools.partial(dispatch_kernel, (E, T, X, C, F, N)), ou...  66 us
    pallas_call x1, Pallas kernels, send_home(): pl.pallas_call(functools.partial(return_kernel, (E, T, C, F)), out_shape=...  31.3 us
    dot_general x1, matrix products, shards(): grad_gate = jnp.dot(grad_pre_gate.T, rows_x, preferred_element_type=F32)  5.31 us
    dot_general x1, matrix products, shards(): lax.dot_general(rows_x, up_mat, contract_last, preferred_element_type=F32)  4.68 us
    unnamed x25, local copies, waits for them, and re-layouts  4.57 us
    dot_general x1, matrix products, shards(): lax.dot_general(rows_g, down_mat, contract_last, preferred_element_type=F32)  3.95 us
    dot_general x1, matrix products, shards(): grad_down = jnp.dot(hidden.T, weighted_cotan, preferred_element_type=F32)  3.42 us
    dot_general x1, matrix products, shards(): grad_up = jnp.dot(grad_pre_up.T, rows_x, preferred_element_type=F32)  3.29 us

profile of v2, /device:TPU:0, one launch (start us, length us, event | category | flops | bytes accessed | tf_op | source)
XLA Modules:
  0.0 137.4 jit_solution(13576513283007859038)
XLA Ops:
  0.6 0.0 copy-start
  0.6 0.9 copy.33
  1.6 0.1 eq.91
  1.7 0.2 fusion.10
  1.9 0.1 convert_element_type.60
  2.1 0.1 copy.34
  2.1 0.7 multiply_add_fusion.1
  2.9 1.3 convolution_convert_fusion
  4.2 0.8 slice_bitcast_fusion
  4.9 0.2 select_reduce_fusion.2
  5.1 0.1 add.38
  5.2 0.2 select_convert_fusion
  5.4 0.1 or_convert_fusion
  5.6 1.1 copy.35
  6.7 0.0 copy-start.4
  6.7 0.9 copy-done.4
  7.7 66.0 %dispatch.1 = (bf16[384,4096]{1,0:T(8,128)(2,1)}, bf16[384,4096]{1,0:T(8,128)(2,1)}, bf16[8,48,256]{2,1,0:T(8,128)(2,1)S(1)}, bf16[8,128,1024]{2,1,0:T(8,128)(2,1)S(1)}, bf16[128,1024]{1,0:T(8,128)(2,1)S(1)}) custom-call(bf16[8,48,1024]{2,1,0:T(8,128)(2,1)S(1)} %bitcast.51, bf16[8,48,256]{2,1,0:T(8,128)(2,1)S(1)} %pad_maximum_fusion.meta_ref, ...), custom_call_target="tpu_custom_call" | custom-call | tf_op jit(solution)/shard_map/dispatch/pallas_call | solution.py:293
  73.7 0.0 copy-start.2
  73.7 0.0 copy-start.5
  73.7 0.0 copy-start.7
  73.7 4.7 %fusion.6 = f32[384,256]{0,1:T(8,128)S(1)} fusion(bf16[384,4096]{1,0:T(8,128)(2,1)} %get-tuple-element.15, bf16[1,256,4096]{2,1,0:T(8,128)(2,1)} %param.13), kind=kOutput, calls=%fused_computation.11 | convolution fusion | flops 805306368 | bytes 5636096 | tf_op jit(solution)/shard_map/dot_general | solution.py:585
  78.4 0.0 copy-done
  78.4 0.0 copy-done.7
  78.4 2.0 %fusion.3 = f32[384,256]{0,1:T(8,128)} fusion(bf16[384,4096]{1,0:T(8,128)(2,1)S(1)} %copy-done.7, bf16[1,256,4096]{2,1,0:T(8,128)(2,1)S(1)} %copy-done), kind=kOutput, calls=%fused_computation.8 | convolution fusion | flops 805306368 | bytes 5636096 | tf_op jit(solution)/shard_map/dot_general | solution.py:584
  80.4 0.0 copy-done.2
  80.4 0.0 copy-done.5
  80.4 0.1 fusion.20
  80.5 0.1 copy.39
  80.6 0.1 copy.38
  80.8 3.9 %multiply_reduce_fusion = (f32[384]{0:T(512)S(1)}, bf16[384,256]{0,1:T(8,128)(2,1)S(1)}, bf16[384,256]{0,1:T(8,128)(2,1)S(1)}, bf16[384,256]{0,1:T(8,128)(2,1)S(1)}) fusion(f32[384,256]{0,1:T(8,128)S(1)} %fusion.6, f32[384,256]{0,1:T(8,128)} %fusion.3, f32[384]{0:T(512)S(1)} %add_reduce_fusion, bf16[384,4096]{1,0:T(8,128)(2,1)} %get-tuple-element.14, ...), kind=kOutput, calls=%fused_computation.19 | convolution fusion | flops 807173760 | bytes 6622208 | tf_op jit(solution)/shard_map/dot_general | solution.py:589
  84.7 0.0 copy-start.10
  84.7 1.0 fusion.1
  85.8 0.6 copy-done.10
  86.3 2.7 %add_convert_fusion.part = bf16[384,4096]{1,0:T(8,128)(2,1)} fusion(f32[384,4096]{1,0:T(8,128)S(1)} %fusion.1, bf16[384,256]{0,1:T(8,128)(2,1)S(1)} %get-tuple-element.25, bf16[1,256,4096]{2,1,0:T(8,128)(2,1)S(1)} %copy-done.10), kind=kOutput, calls=%fused_computation.1 | convolution fusion | flops 808452096 | bytes 11730944 | tf_op jit(solution)/shard_map/dot_general | solution.py:601
  89.0 0.1 reshape.114
  89.1 0.0 copy-start.1
  89.1 1.9 %copy-done.1 = bf16[384,4096]{1,0:T(8,128)(2,1)S(1)} copy-done((bf16[384,4096]{1,0:T(8,128)(2,1)S(1)}, bf16[384,4096]{1,0:T(8,128)(2,1)}, u32[]{:S(2)}) %copy-start.1) | copy-done | bytes 3145752
  91.0 31.3 %send_home.1 = (bf16[8,48,1024]{2,1,0:T(8,128)(2,1)S(1)}, f32[8,8,128]{2,1,0:T(8,128)S(1)}) custom-call(bf16[384,4096]{1,0:T(8,128)(2,1)S(1)} %copy-done.1, f32[8,8,128]{2,1,0:T(8,128)S(1)} %pad.4.gate), custom_call_target="tpu_custom_call" | custom-call | tf_op jit(solution)/shard_map/send_home/pallas_call | solution.py:506
  122.3 1.1 convolution_convert_fusion.1
  123.4 0.1 broadcast_in_dim.100
  123.4 0.1 select_reduce_fusion.1
  123.6 0.6 pad_maximum_fusion.1
  124.2 0.0 copy-start.8
  124.2 5.3 %convolution_bitcast_fusion.2 = f32[1,256,4096]{2,1,0:T(8,128)} fusion(bf16[384,256]{0,1:T(8,128)(2,1)S(1)} %get-tuple-element.24, bf16[384,4096]{1,0:T(8,128)(2,1)} %get-tuple-element.15), kind=kOutput, calls=%fused_computation.4 | convolution fusion | flops 805306368 | bytes 7536640 | tf_op jit(solution)/shard_map/dot_general | solution.py:598
  129.5 0.0 copy-done.8
  129.5 0.0 copy-start.9
  129.5 3.3 %convolution_bitcast_fusion.1 = f32[1,256,4096]{2,1,0:T(8,128)} fusion(bf16[384,256]{0,1:T(8,128)(2,1)S(1)} %get-tuple-element.25, bf16[384,4096]{1,0:T(8,128)(2,1)S(1)} %copy-done.8), kind=kOutput, calls=%fused_computation.3 | convolution fusion | flops 805306368 | bytes 7536640 | tf_op jit(solution)/shard_map/dot_general | solution.py:599
  132.8 0.0 copy-done.9
  132.8 0.0 copy-start.3
  132.8 0.0 copy-start.6
  132.8 3.4 %convolution_bitcast_fusion = f32[1,256,4096]{2,1,0:T(8,128)} fusion(bf16[384,256]{0,1:T(8,128)(2,1)S(1)} %get-tuple-element.23, bf16[384,4096]{1,0:T(8,128)(2,1)S(1)} %copy-done.9, f32[384]{0:T(512)S(1)} %add_reduce_fusion), kind=kOutput, calls=%fused_computation.2 | convolution fusion | flops 810024960 | bytes 7538176 | tf_op jit(solution)/shard_map/dot_general | solution.py:597
  136.2 0.0 copy-done.3
  136.2 0.0 copy-done.6
  136.2 1.2 fusion.22
  (10 shorter events, 0.1 us)
Async XLA Ops:
  0.6 77.7 %copy-start = (bf16[1,256,4096]{2,1,0:T(8,128)(2,1)S(1)}, bf16[1,256,4096]{2,1,0:T(8,128)(2,1)}, u32[]{:S(2)}) copy-start(bf16[1,256,4096]{2,1,0:T(8,128)(2,1)} %param.12) | copy-start | bytes 6291460
  6.7 1.0 copy-start.4
  73.7 6.8 %copy-start.2 = (bf16[8,128,1024]{2,1,0:T(8,128)(2,1)}, bf16[8,128,1024]{2,1,0:T(8,128)(2,1)S(1)}, u32[]{:S(2)}) copy-start(bf16[8,128,1024]{2,1,0:T(8,128)(2,1)S(1)} %get-tuple-element.19) | copy-start | bytes 6291460
  73.7 6.8 %copy-start.5 = (bf16[128,1024]{1,0:T(8,128)(2,1)}, bf16[128,1024]{1,0:T(8,128)(2,1)S(1)}, u32[]{:S(2)}) copy-start(bf16[128,1024]{1,0:T(8,128)(2,1)S(1)} %get-tuple-element.18) | copy-start | bytes 786436
  73.7 4.7 %copy-start.7 = (bf16[384,4096]{1,0:T(8,128)(2,1)S(1)}, bf16[384,4096]{1,0:T(8,128)(2,1)}, u32[]{:S(2)}) copy-start(bf16[384,4096]{1,0:T(8,128)(2,1)} %get-tuple-element.15) | copy-start | bytes 9437188
  84.7 1.6 %copy-start.10 = (bf16[1,256,4096]{2,1,0:T(8,128)(2,1)S(1)}, bf16[1,256,4096]{2,1,0:T(8,128)(2,1)}, u32[]{:S(2)}) copy-start(bf16[1,256,4096]{2,1,0:T(8,128)(2,1)} %param.13) | copy-start | bytes 6291460
  89.1 1.9 %copy-start.1 = (bf16[384,4096]{1,0:T(8,128)(2,1)S(1)}, bf16[384,4096]{1,0:T(8,128)(2,1)}, u32[]{:S(2)}) copy-start(bf16[384,4096]{1,0:T(8,128)(2,1)} %add_convert_fusion.part) | copy-start | bytes 9437188
  124.2 5.3 %copy-start.8 = (bf16[384,4096]{1,0:T(8,128)(2,1)S(1)}, bf16[384,4096]{1,0:T(8,128)(2,1)}, u32[]{:S(2)}) copy-start(bf16[384,4096]{1,0:T(8,128)(2,1)} %get-tuple-element.15) | copy-start | bytes 9437188
  129.5 3.3 %copy-start.9 = (bf16[384,4096]{1,0:T(8,128)(2,1)S(1)}, bf16[384,4096]{1,0:T(8,128)(2,1)}, u32[]{:S(2)}) copy-start(bf16[384,4096]{1,0:T(8,128)(2,1)} %get-tuple-element.14) | copy-start | bytes 9437188
  132.8 3.4 %copy-start.3 = (bf16[8,128,1024]{2,1,0:T(8,128)(2,1)S(1)}, bf16[8,128,1024]{2,1,0:T(8,128)(2,1)}, u32[]{:S(2)}) copy-start(bf16[8,128,1024]{2,1,0:T(8,128)(2,1)} %copy-done.2) | copy-start | bytes 6291460
  132.8 3.4 %copy-start.6 = (bf16[128,1024]{1,0:T(8,128)(2,1)S(1)}, bf16[128,1024]{1,0:T(8,128)(2,1)}, u32[]{:S(2)}) copy-start(bf16[128,1024]{1,0:T(8,128)(2,1)} %copy-done.5) | copy-start | bytes 786436

commit v3 on v2

--- a/solution.py
+++ b/solution.py
@@ -60,12 +60,11 @@
         return 0
 
     lax.fori_loop(1, E, greet, 0)
-    for dy in range(1, Y):
+    for dt in range(1, T):
         pl.semaphore_signal(
-            barrier, inc=1, device_id=(me, ((y + dy) % Y) * 2 + c), device_id_type=MESH
-        )
-    pl.semaphore_signal(barrier, inc=1, device_id=(me, sib), device_id_type=MESH)
-    pl.semaphore_wait(barrier, (E - 1) + (Y - 1) + 1)
+            barrier, inc=1, device_id=(me, (tp + dt) % T), device_id_type=MESH
+        )
+    pl.semaphore_wait(barrier, (E - 1) + (T - 1))
 
     def rows_of(s):
         return pl.ds(pl.multiple_of(s * C, 16), C)
@@ -281,48 +280,6 @@
             cp = remote(other, other, sib_send.at[a, dy], sib_recv.at[a, dy], (me, sib))
             cp.wait_send()
             cp.wait_recv()
-
-
-def dispatch(E, T, C, F, N, rows, meta, cotangent, shared):
-    X = 2 if E % 2 == 0 else 1
-    Y = T // 2
-    S = shared.shape[1]
-    M = meta.shape[2]
-    dma = pltpu.SemaphoreType.DMA
-    vmem = pl.BlockSpec(memory_space=pltpu.VMEM)
-    return pl.pallas_call(
-        functools.partial(dispatch_kernel, (E, T, X, C, F, N)),
-        out_shape=(
-            jax.ShapeDtypeStruct((E * C, T * F), BF16),
-            jax.ShapeDtypeStruct((E * C, T * F), BF16),
-            jax.ShapeDtypeStruct((E, C, M), BF16),
-            jax.ShapeDtypeStruct((E, N, F), BF16),
-            jax.ShapeDtypeStruct((S, E * N), BF16),
-        ),
-        in_specs=[vmem] * 4,
-        out_specs=(vmem,) * 5,
-        scratch_shapes=[
-            dma((4,)),
-            dma((E,)),
-            dma((E,)),
-            dma((E,)),
-            dma((E,)),
-            dma((E,)),
-            dma((E,)),
-            dma((E,)),
-            dma((E,)),
-            dma((max(X - 1, 1), E)),
-            dma((E,)),
-            dma((2, max(Y - 1, 1))),
-            dma((2, max(Y - 1, 1), E)),
-            dma((2, Y)),
-            dma((2, Y)),
-        ],
-        compiler_params=pltpu.CompilerParams(
-            collective_id=0, has_side_effects=True, vmem_limit_bytes=48 * 1024 * 1024
-        ),
-        name="dispatch",
-    )(rows, meta, cotangent, shared)
 
 
 def return_kernel(
@@ -356,21 +313,6 @@
     c = tp % 2
     sib = y * 2 + (1 - c)
 
-    barrier = pltpu.get_barrier_semaphore()
-
-    def greet(d, _):
-        pl.semaphore_signal(
-            barrier, inc=1, device_id=((me + d) % E, tp), device_id_type=MESH
-        )
-        return 0
-
-    lax.fori_loop(1, E, greet, 0)
-    for dt in range(1, T):
-        pl.semaphore_signal(
-            barrier, inc=1, device_id=(me, (tp + dt) % T), device_id_type=MESH
-        )
-    pl.semaphore_wait(barrier, (E - 1) + (T - 1))
-
     def rows_of(s):
         return pl.ds(pl.multiple_of(s * C, 16), C)
 
@@ -498,42 +440,191 @@
     done.wait_recv()
 
 
-def send_home(E, T, C, F, part, gate):
+def expert_compute(
+    dims, xfull, gfull, meta_out, hidden, grad_gate, grad_up, wg, wu, wd, accs, part, gate
+):
+    E, T, C, F, N = dims
+    acc_g, acc_u, acc_b = accs.at[0], accs.at[1], accs.at[2]
+    nt = (((1,), (1,)), ((), ()))
+    accs[...] = jnp.zeros_like(accs)
+
+    def forward(t, _):
+        cols = pl.ds(pl.multiple_of(t * F, 128), F)
+        acc_g[...] += lax.dot_general(
+            xfull[:, cols], wg[:, cols], nt, preferred_element_type=F32
+        )
+        acc_u[...] += lax.dot_general(
+            xfull[:, cols], wu[:, cols], nt, preferred_element_type=F32
+        )
+        acc_b[...] += lax.dot_general(
+            gfull[:, cols], wd[:, cols], nt, preferred_element_type=F32
+        )
+        return 0
+
+    lax.fori_loop(0, T, forward, 0)
+    diagonal = lax.broadcasted_iota(jnp.int32, (C, 128), 0) == lax.broadcasted_iota(
+        jnp.int32, (C, 128), 1
+    )
+
+    def middle(s, _):
+        rows = pl.ds(pl.multiple_of(s * C, 16), C)
+        pre_gate = acc_g[rows, :]
+        pre_up = acc_u[rows, :]
+        back = acc_b[rows, :]
+        weight = meta_out[s, :, N : N + 128].astype(F32)
+        weight = weight[:, 0:1] + weight[:, 1:2]
+        sigmoid_gate = jax.nn.sigmoid(pre_gate)
+        silu_gate = pre_gate * sigmoid_gate
+        hid = (silu_gate * pre_up).astype(BF16)
+        hidden[rows, :] = hid
+        column = jnp.sum(hid.astype(F32) * back, axis=1, keepdims=True)
+        line = jnp.sum(jnp.where(diagonal, column, 0.0), axis=0, keepdims=True)
+        gate[s] = jnp.broadcast_to(line, (8, 128))
+        scaled = weight * back
+        grad_gate[rows, :] = (
+            scaled * pre_up * sigmoid_gate * (1.0 + pre_gate * (1.0 - sigmoid_gate))
+        ).astype(BF16)
+        grad_up[rows, :] = (scaled * silu_gate).astype(BF16)
+        return 0
+
+    lax.fori_loop(0, E, middle, 0)
+
+    def partial(t, _):
+        cols = pl.ds(pl.multiple_of(t * F, 128), F)
+        part[:, cols] = (
+            jnp.dot(grad_gate[...], wg[:, cols], preferred_element_type=F32)
+            + jnp.dot(grad_up[...], wu[:, cols], preferred_element_type=F32)
+        ).astype(BF16)
+        return 0
+
+    lax.fori_loop(0, T, partial, 0)
+
+
+def whole_kernel(dims, n_dispatch, *refs):
+    E, T, X, C, F, N = dims
+    tok, meta, cot, sh, w_gate, w_up, w_down = refs[:7]
+    xfull, gfull, meta_out, cot_all, sh_out, hidden, grad_gate, grad_up, back, gate_back = refs[
+        7:17
+    ]
+    wg, wu, wd, accs, part, gate, load_sem = refs[17:24]
+    rest = refs[24:]
+    loads = [
+        pltpu.make_async_copy(src.at[0], dst, load_sem.at[i])
+        for i, (src, dst) in enumerate(((w_gate, wg), (w_up, wu), (w_down, wd)))
+    ]
+    for cp in loads:
+        cp.start()
+    dispatch_kernel(
+        dims,
+        tok,
+        meta,
+        cot,
+        sh,
+        xfull,
+        gfull,
+        meta_out,
+        cot_all,
+        sh_out,
+        *rest[:n_dispatch],
+    )
+    for cp in loads:
+        cp.wait()
+    expert_compute(
+        (E, T, C, F, N),
+        xfull,
+        gfull,
+        meta_out,
+        hidden,
+        grad_gate,
+        grad_up,
+        wg,
+        wu,
+        wd,
+        accs,
+        part,
+        gate,
+    )
+    return_kernel((E, T, C, F), part, gate, back, gate_back, *rest[n_dispatch:])
+
+
+def routed(E, T, C, F, N, rows, meta, cotangent, shared, w_gate, w_up, w_down):
+    X = 2 if E % 2 == 0 else 1
     Y = T // 2
+    Z = max(Y - 1, 1)
     R = E * C
+    S = shared.shape[1]
+    H = w_gate.shape[1]
     dma = pltpu.SemaphoreType.DMA
     vmem = pl.BlockSpec(memory_space=pltpu.VMEM)
+    anywhere = pl.BlockSpec(memory_space=pl.ANY)
+    shape = jax.ShapeDtypeStruct
+    sems = [
+        dma((4,)),
+        dma((E,)),
+        dma((E,)),
+        dma((E,)),
+        dma((E,)),
+        dma((E,)),
+        dma((E,)),
+        dma((E,)),
+        dma((E,)),
+        dma((max(X - 1, 1), E)),
+        dma((E,)),
+        dma((2, Z)),
+        dma((2, Z, E)),
+        dma((2, Y)),
+        dma((2, Y)),
+    ]
+    home = [
+        pltpu.VMEM((Y, R, F), BF16),
+        pltpu.VMEM((Z, R, F), BF16),
+        pltpu.VMEM((Z, R, F), BF16),
+        pltpu.VMEM((R, F), BF16),
+        pltpu.VMEM((T, E, 8, 128), F32),
+        pltpu.VMEM((E, 8, 128), F32),
+        dma((Y,)),
+        dma((Y, E)),
+        dma((Z,)),
+        dma((Z, E)),
+        dma,
+        dma,
+        dma((T,)),
+        dma((T,)),
+        dma,
+        dma,
+    ]
     return pl.pallas_call(
-        functools.partial(return_kernel, (E, T, C, F)),
+        functools.partial(whole_kernel, (E, T, X, C, F, N), len(sems)),
         out_shape=(
-            jax.ShapeDtypeStruct((E, C, F), BF16),
-            jax.ShapeDtypeStruct(gate.shape, F32),
+            shape((R, T * F), BF16),
+            shape((R, T * F), BF16),
+            shape(meta.shape, BF16),
+            shape((E, N, F), BF16),
+            shape((S, E * N), BF16),
+            shape((R, H), BF16),
+            shape((R, H), BF16),
+            shape((R, H), BF16),
+            shape((E, C, F), BF16),
+            shape((E, 8, 128), F32),
         ),
-        in_specs=[vmem] * 2,
-        out_specs=(vmem,) * 2,
+        in_specs=[vmem] * 4 + [anywhere] * 3,
+        out_specs=(vmem,) * 10,
         scratch_shapes=[
-            pltpu.VMEM((Y, R, F), BF16),
-            pltpu.VMEM((max(Y - 1, 1), R, F), BF16),
-            pltpu.VMEM((max(Y - 1, 1), R, F), BF16),
-            pltpu.VMEM((R, F), BF16),
-            pltpu.VMEM((T,) + gate.shape, F32),
-            pltpu.VMEM(gate.shape, F32),
-            dma((Y,)),
-            dma((Y, E)),
-            dma((max(Y - 1, 1),)),
-            dma((max(Y - 1, 1), E)),
-            dma,
-            dma,
-            dma((T,)),
-            dma((T,)),
-            dma,
-            dma,
-        ],
+            pltpu.VMEM((H, T * F), BF16),
+            pltpu.VMEM((H, T * F), BF16),
+            pltpu.VMEM((H, T * F), BF16),
+            pltpu.VMEM((3, R, H), F32),
+            pltpu.VMEM((R, T * F), BF16),
+            pltpu.VMEM((E, 8, 128), F32),
+            dma((3,)),
+        ]
+        + sems
+        + home,
         compiler_params=pltpu.CompilerParams(
-            collective_id=1, has_side_effects=True, vmem_limit_bytes=40 * 1024 * 1024
+            collective_id=0, has_side_effects=True, vmem_limit_bytes=56 * 1024 * 1024
         ),
-        name="send_home",
-    )(part, gate)
+        name="routed",
+    )(rows, meta, cotangent, shared, w_gate, w_up, w_down)
 
 
 def shards(tokens, cotangent, routes, gate_weight, w_gate, w_up, w_down, shared_hidden):
@@ -570,40 +661,31 @@
     rows = jnp.dot(select, tokens, preferred_element_type=F32).astype(BF16).reshape(E, C, F)
     shared = shared_hidden.T.reshape(E, shared_hidden.shape[1] // E, tok_count)
 
-    rows_x, rows_g, meta_got, cot_all, shared_got = dispatch(
-        E, T, C, F, tok_count, rows, meta, cotangent, shared
+    (
+        rows_x,
+        rows_g,
+        meta_got,
+        cot_all,
+        shared_got,
+        hidden,
+        grad_pre_gate,
+        grad_pre_up,
+        back_rows,
+        back_gate,
+    ) = routed(
+        E, T, C, F, tok_count, rows, meta, cotangent, shared, w_gate, w_up, w_down
     )
     got = meta_got.reshape(R, tok_count + 128)
     weight_col = got[:, tok_count : tok_count + 1].astype(F32) + got[
         :, tok_count + 1 : tok_count + 2
     ].astype(F32)
-    contract_last = (((1,), (1,)), ((), ()))
-    gate_mat = w_gate[0]
-    up_mat = w_up[0]
-    down_mat = w_down[0]
-    pre_gate = lax.dot_general(rows_x, gate_mat, contract_last, preferred_element_type=F32)
-    pre_up = lax.dot_general(rows_x, up_mat, contract_last, preferred_element_type=F32)
-    sigmoid_gate = jax.nn.sigmoid(pre_gate)
-    silu_gate = pre_gate * sigmoid_gate
-    hidden = (silu_gate * pre_up).astype(BF16)
-    back_hidden = lax.dot_general(rows_g, down_mat, contract_last, preferred_element_type=F32)
-    gate_part = jnp.sum(hidden.astype(F32) * back_hidden, axis=1)
-    scaled = weight_col * back_hidden
-    grad_pre_gate = (
-        scaled * pre_up * sigmoid_gate * (1.0 + pre_gate * (1.0 - sigmoid_gate))
-    ).astype(BF16)
-    grad_pre_up = (scaled * silu_gate).astype(BF16)
     weighted_cotan = (weight_col * rows_g.astype(F32)).astype(BF16)
     grad_down = jnp.dot(hidden.T, weighted_cotan, preferred_element_type=F32)
     grad_gate = jnp.dot(grad_pre_gate.T, rows_x, preferred_element_type=F32)
     grad_up = jnp.dot(grad_pre_up.T, rows_x, preferred_element_type=F32)
-    partial_value = jnp.dot(grad_pre_gate, gate_mat, preferred_element_type=F32)
-    partial_value = partial_value + jnp.dot(grad_pre_up, up_mat, preferred_element_type=F32)
     shared_grad = jnp.dot(
         shared_got, cot_all.reshape(E * tok_count, F), preferred_element_type=F32
     )
-    gate_box = jnp.pad(gate_part.reshape(E, 1, C), ((0, 0), (0, 7), (0, 128 - C)))
-    back_rows, back_gate = send_home(E, T, C, F, partial_value.astype(BF16), gate_box)
     back_gate = back_gate[:, 0, :C]
     tokens_grad = lax.dot_general(
         select, back_rows.reshape(R, F), (((0,), (0,)), ((), ())), preferred_element_type=F32

time: 138 us -> 131 us (0.949)
  matrix products: 30.2 us -> 17.8 us
  Pallas kernels: 97.3 us -> 102 us
    dot_general x5 -> x0, matrix products: 14.4 us -> none  [the longest x1 4.68 us: shards(): lax.dot_general(rows_x, up_mat, contract_last, preferred_element_type=F32)]
    pallas_call x2 -> x1, Pallas kernels: 97.3 us -> 102 us  [routed(): pl.pallas_call(functools.partial(whole_kernel, (E, T, X, C, F, N), len(se...]
    unnamed x25 -> x13, local copies, waits for them, and re-layouts: 4.57 us -> 1.89 us
    dot_general x1, matrix products: 5.31 us -> 3.3 us  [shards(): grad_gate = jnp.dot(grad_pre_gate.T, rows_x, preferred_element_type=F32)]
    dot_general x1, matrix products: 1.24 us -> 2.94 us  [shards(): jnp.dot(shared_got, cot_all.reshape(E * tok_count, F), preferred_element_...]
    slice x1, local copies, waits for them, and re-layouts: 0.1 us -> 1.63 us  [shards(): got[:, tok_count:tok_count + 1].astype(F32)]
where the time goes in v3:
time: 131 us
  Pallas kernels  102 us (78%)
  matrix products  17.8 us (14%)
  local copies, waits for them, and re-layouts  7.33 us (6%)
  other arithmetic  2.67 us (2%)
    pallas_call x1, Pallas kernels, routed(): pl.pallas_call(functools.partial(whole_kernel, (E, T, X, C, F, N), len(se...  102 us
    dot_general x1, matrix products, shards(): grad_down = jnp.dot(hidden.T, weighted_cotan, preferred_element_type=F32)  4.45 us
    dot_general x1, matrix products, shards(): grad_up = jnp.dot(grad_pre_up.T, rows_x, preferred_element_type=F32)  3.3 us
    dot_general x1, matrix products, shards(): grad_gate = jnp.dot(grad_pre_gate.T, rows_x, preferred_element_type=F32)  3.3 us
    dot_general x1, matrix products, shards(): jnp.dot(shared_got, cot_all.reshape(E * tok_count, F), preferred_element_...  2.94 us

profile of v3, /device:TPU:0, one launch (start us, length us, event | category | flops | bytes accessed | tf_op | source)
XLA Modules:
  0.0 131.0 jit_solution(4307778915708525839)
XLA Ops:
  0.6 0.0 copy-start
  0.6 0.8 slice_bitcast_fusion
  1.4 0.8 copy.33
  2.2 0.1 eq.91
  2.3 0.2 fusion.1
  2.6 0.1 convert_element_type.43
  2.7 0.1 copy.34
  2.8 0.7 multiply_add_fusion.1
  3.5 0.2 select_reduce_fusion.2
  3.7 0.1 add.27
  3.8 0.2 select_convert_fusion
  3.9 0.1 or_convert_fusion
  4.1 0.7 pad_maximum_fusion.refs_1_
  4.8 1.8 %copy.35 = bf16[1024,128]{1,0:T(8,128)(2,1)} copy(bf16[1024,128]{0,1:T(8,128)(2,1)} %bitcast.35) | data formatting | bytes 524288 | tf_op jit(solution)/shard_map/transpose | solution.py:662
  6.6 0.0 copy-done
  6.6 1.2 convolution_convert_fusion
  7.8 102.5 %routed.1 = (bf16[384,4096]{1,0:T(8,128)(2,1)}, bf16[384,4096]{1,0:T(8,128)(2,1)}, bf16[8,48,256]{2,1,0:T(8,128)(2,1)}, bf16[8,128,1024]{2,1,0:T(8,128)(2,1)}, b...) custom-call(bf16[8,48,1024]{2,1,0:T(8,128)(2,1)} %bitcast.31, ...), custom_call_target="tpu_custom_call" | custom-call | tf_op jit(solution)/shard_map/routed/pallas_call | solution.py:596
  110.3 0.0 copy-start.2
  110.3 2.3 %convolution_convert_fusion.1 = bf16[128,1024]{1,0:T(8,128)(2,1)} fusion(bf16[384,1024]{1,0:T(8,128)(2,1)} %bitcast.34, s32[128]{0:T(128)S(1)} %get-tuple-element.35, s32[128]{0:T(128)S(1)} %get-tuple-element.34), kind=kOutput, calls=%fused_computation.6 | convolution fusion | flops 100941824 | bytes 1049600 | tf_op jit(solution)/shard_map/dot_general | solution.py:690
  112.6 0.8 slice_reduce_fusion
  113.4 0.1 broadcast_in_dim.100
  113.5 0.1 select_reduce_fusion.1
  113.6 0.6 pad_maximum_fusion.1
  114.2 1.6 %fusion.10 = (bf16[384,1]{1,0:T(8,128)(2,1)}, bf16[384,1]{1,0:T(8,128)(2,1)S(1)}) fusion(bf16[384,256]{1,0:T(8,128)(2,1)} %bitcast.36), kind=kLoop, calls=%fused_computation.39 | loop fusion | bytes 3072 | tf_op jit(solution)/shard_map/slice | solution.py:679
  115.8 1.0 copy.38
  116.8 0.1 copy.39
  116.9 2.9 %fusion.12 = f32[128,1024]{1,0:T(8,128)} fusion(bf16[128,1024]{1,0:T(8,128)(2,1)} %get-tuple-element.24, bf16[1024,1024]{1,0:T(8,128)(2,1)} %bitcast.32), kind=kOutput, calls=%fused_computation.41 | convolution fusion | flops 268435456 | bytes 2883584 | tf_op jit(solution)/shard_map/dot_general | solution.py:686
  119.9 0.0 copy-done.2
  119.9 0.0 copy-start.1
  119.9 0.0 copy-start.4
  119.9 4.4 %convolution_bitcast_fusion = f32[1,256,4096]{2,1,0:T(8,128)} fusion(bf16[384,256]{1,0:T(8,128)(2,1)} %get-tuple-element.21, bf16[384,4096]{1,0:T(8,128)(2,1)S(1)} %copy-done.2, f32[384]{0:T(512)S(1)} %add_reduce_fusion), kind=kOutput, calls=%fused_computation.1 | convolution fusion | flops 810024960 | bytes 7538176 | tf_op jit(solution)/shard_map/dot_general | solution.py:683
  124.3 0.0 copy-done.1
  124.3 0.0 copy-done.4
  124.3 0.0 copy-start.3
  124.3 3.3 %convolution_bitcast_fusion.2 = f32[1,256,4096]{2,1,0:T(8,128)} fusion(bf16[384,256]{1,0:T(8,128)(2,1)S(1)} %copy-done.4, bf16[384,4096]{1,0:T(8,128)(2,1)S(1)} %copy-done.1), kind=kOutput, calls=%fused_computation.3 | convolution fusion | flops 805306368 | bytes 7536640 | tf_op jit(solution)/shard_map/dot_general | solution.py:684
  127.7 0.0 copy-done.3
  127.7 3.3 %convolution_bitcast_fusion.1 = f32[1,256,4096]{2,1,0:T(8,128)} fusion(bf16[384,256]{1,0:T(8,128)(2,1)S(1)} %copy-done.3, bf16[384,4096]{1,0:T(8,128)(2,1)S(1)} %copy-done.1), kind=kOutput, calls=%fused_computation.2 | convolution fusion | flops 805306368 | bytes 7536640 | tf_op jit(solution)/shard_map/dot_general | solution.py:685
  (7 shorter events, 0.1 us)
Async XLA Ops:
  0.6 5.9 %copy-start = (bf16[128,1024]{1,0:T(8,128)(2,1)S(1)}, bf16[128,1024]{1,0:T(8,128)(2,1)}, u32[]{:S(2)}) copy-start(bf16[128,1024]{1,0:T(8,128)(2,1)} %param.8) | copy-start | bytes 786436
  110.3 9.6 %copy-start.2 = (bf16[384,4096]{1,0:T(8,128)(2,1)S(1)}, bf16[384,4096]{1,0:T(8,128)(2,1)}, u32[]{:S(2)}) copy-start(bf16[384,4096]{1,0:T(8,128)(2,1)} %get-tuple-element.23) | copy-start | bytes 9437188
  119.9 4.5 %copy-start.1 = (bf16[384,4096]{1,0:T(8,128)(2,1)S(1)}, bf16[384,4096]{1,0:T(8,128)(2,1)}, u32[]{:S(2)}) copy-start(bf16[384,4096]{1,0:T(8,128)(2,1)} %get-tuple-element.19) | copy-start | bytes 9437188
  119.9 4.5 %copy-start.4 = (bf16[384,256]{1,0:T(8,128)(2,1)S(1)}, bf16[384,256]{1,0:T(8,128)(2,1)}, u32[]{:S(2)}) copy-start(bf16[384,256]{1,0:T(8,128)(2,1)} %get-tuple-element.18) | copy-start | bytes 589828
  124.3 3.3 %copy-start.3 = (bf16[384,256]{1,0:T(8,128)(2,1)S(1)}, bf16[384,256]{1,0:T(8,128)(2,1)}, u32[]{:S(2)}) copy-start(bf16[384,256]{1,0:T(8,128)(2,1)} %get-tuple-element.20) | copy-start | bytes 589828
